TPU v7x, 32 devices: a whole 2x2x4 slice. The times are simulated.
32 devices in a mesh: grp: 2 (over x), ep: 16 (over z, y, core).
Axes of the slice: x: 2, y: 2, z: 4, core: 2. Of those that a mesh axis runs over, the one named last changes fastest.
Arguments:
- hidden: bfloat16 [224, 2048], P(('grp', 'ep')), parts along dimension 0, may hold values from -6 to 6
- state_in: float32 [224, 64, 4096], P(('grp', 'ep')), parts along dimension 0, may hold values from -4 to 4
- conv_state: bfloat16 [224, 3, 4608], P(('grp', 'ep')), parts along dimension 0, may hold values from -6 to 6
- expert_ids: int32 [224, 4], P(('grp', 'ep')), parts along dimension 0, may hold values from 0 to 15, as said below
- group_prob: float32 [224], P(('grp', 'ep')), parts along dimension 0, may hold values from 0.25 to 1
- expert_score: float32 [224, 4], P(('grp', 'ep')), parts along dimension 0, may hold values from 0.05 to 1
- first_gain: bfloat16 [2048], replicated, may hold values from 0.099609375 to 1.8984375
- z_weight: bfloat16 [2048, 4096], P(None, 'ep'), may hold values from -0.125 to 0.125
- x_weight: bfloat16 [2048, 4096], P(None, 'ep'), may hold values from -0.125 to 0.125
- b_weight: bfloat16 [2048, 256], replicated, may hold values from -0.125 to 0.125
- c_weight: bfloat16 [2048, 256], replicated, may hold values from -0.125 to 0.125
- dt_weight: bfloat16 [2048, 64], replicated, may hold values from -0.125 to 0.125
- conv_weight: bfloat16 [4, 4608], replicated, may hold values from -3 to 3
- conv_bias: bfloat16 [4608], replicated, may hold values from -3 to 3
- dt_bias: float32 [64], replicated, may hold values from -4 to 0
- decay_log: float32 [64], replicated, may hold values from 0 to 2
- skip_gain: float32 [64], replicated, may hold values from 0.1 to 1.9
- inner_gain: bfloat16 [4096], replicated, may hold values from 0.099609375 to 1.8984375
- out_weight: bfloat16 [4096, 2048], P(None, 'ep'), may hold values from -0.09375 to 0.09375
- second_gain: bfloat16 [2048], replicated, may hold values from 0.099609375 to 1.8984375
- expert_gate: bfloat16 [16, 2048, 512], P('ep'), may hold values from -0.125 to 0.125
- expert_up: bfloat16 [16, 2048, 512], P('ep'), may hold values from -0.125 to 0.125
- expert_down: bfloat16 [16, 512, 2048], P('ep'), may hold values from -0.25 to 0.25
Outputs:
- layer_out: bfloat16 [224, 2048], P(('grp', 'ep')), parts along dimension 0
- state_out: float32 [224, 64, 4096], P(('grp', 'ep')), parts along dimension 0
- conv_out: bfloat16 [224, 3, 4608], P(('grp', 'ep')), parts along dimension 0
There are 2 independent parts, one for each index of `grp`. A program takes and returns all parts, laid end to end along the dimension named above; an argument that names none is the same for every part. Nothing has to cross between parts.
Inputs may be any that keep to these rules, and one draw needn't show every extreme that they name: `expert_ids`: each row names 4 different experts of one expert group (numbers g * 8 to g * 8 + 7). Among the 7 rows of one device no expert is named more than 3 times, and in every draw one expert is named exactly 3 times by the rows of every device.
All inputs are finite; a program needn't handle non-finite values.
Results may differ from a plain program's by a relative error of at most 0.014.
Values may be sent and summed in bfloat16 or wider, within the bound.
No kernel may reach another device: no remote copies, remote signals or barrier semaphores. Data moves between devices by JAX's collectives and lax.ppermute only.
A program may use at most 128 MiB of HBM per device.

v0:
```python
import functools

import jax
import jax.numpy as jnp
from jax import lax
from jax.experimental import pallas as pl
from jax.experimental.pallas import tpu as pltpu
from jax.sharding import PartitionSpec as P


HEADS = 64
HEAD_DIM = 64
SSM_GROUPS = 4
STATE = 64
TOP = 4
EPS = 1e-06
PAD = 8
LANES = 128
F32 = jnp.float32
BF16 = jnp.bfloat16


def silu(v):
    return v * jax.nn.sigmoid(v)


def call(kernel, out_shape, limit_mib, flops, moved, **kw):
    return pl.pallas_call(
        kernel,
        out_shape=out_shape,
        compiler_params=pltpu.CompilerParams(vmem_limit_bytes=limit_mib * 2**20),
        cost_estimate=pl.CostEstimate(flops=flops, bytes_accessed=moved, transcendentals=0),
        **kw,
    )


def vmem():
    return pl.BlockSpec(memory_space=pltpu.VMEM)


def swap(values, bits, count):
    return lax.ppermute(values, "ep", [(i, i ^ bits) for i in range(count)])


def join_kernel(*refs):
    for k, ref in enumerate(refs[:-1]):
        refs[-1][k] = ref[...]


def join(blocks, shape):
    return call(
        join_kernel,
        jax.ShapeDtypeStruct((len(blocks),) + shape, blocks[0].dtype),
        4,
        blocks[0].size,
        blocks[0].size,
        in_specs=[vmem()] * len(blocks),
        out_specs=vmem(),
        name="join",
    )(*blocks)


def gather(block, count, ahead, local_copy=None):
    blocks = [block if local_copy is None else local_copy]
    for k in reversed(range(1, count // 4)):
        blocks.append(swap(block, 4 * k, count))
    side = []
    for k in range(ahead):
        side.append(swap(blocks[k], 2, count))
    rest = early = join(blocks[ahead:], block.shape)
    rest = swap(rest, 2, count)
    if ahead:
        early = join(blocks + side, block.shape)
    early_core = swap(early, 1, count)
    return early, rest, early_core, swap(rest, 1, count)


def owners(me, parts, count, ahead):
    near = [0] + [4 * k for k in reversed(range(1, count // 4))]
    early = near + [bits ^ 2 for bits in near[:ahead]]
    rest = [bits ^ 2 for bits in near[ahead:]]
    every = early, rest, [bits ^ 1 for bits in early], [bits ^ 1 for bits in rest]
    for bits, part in zip(every, parts):
        for k in range(part.shape[0]):
            yield part, k, me ^ bits[k]


AHEAD = {"first": 0, "second": 2}


def widen_rows(ref, rows):
    groups, _, lanes = ref.shape
    per_group = HEADS // groups
    lines = [
        jnp.broadcast_to(ref[g, t : t + 1, :], (per_group, lanes))
        for t in range(rows)
        for g in range(groups)
    ]
    return jnp.concatenate(lines, axis=0).reshape(rows, HEADS, lanes)


def three_parts(values):
    high = values.astype(BF16)
    rest = values - high.astype(F32)
    mid = rest.astype(BF16)
    low = (rest - mid.astype(F32)).astype(BF16)
    return high, mid, low


def one_row(ref):
    values = ref[...].astype(F32)
    return jnp.concatenate([values[k : k + 1] for k in range(values.shape[0])], axis=1)


def to_column(row, rows):
    size = row.shape[1]
    i = lax.broadcasted_iota(jnp.int32, (rows, size), 0)
    j = lax.broadcasted_iota(jnp.int32, (rows, size), 1)
    return jnp.sum(jnp.where(i == j, jnp.broadcast_to(row, (rows, size)), 0.0), axis=1, keepdims=True)


def local_kernel(
    hidden_ref, gain_ref, b_ref, c_ref, dt_ref, conv_ref, taps_ref, bias_ref, dt_bias_ref,
    log_ref, skip_ref, ids_ref, prob_ref, score_ref,
    early_ref, coef_ref, step_ref, b_wide_ref, c_wide_ref, decay_ref, bc_ref, ids_out_ref, share_ref,
    own_ref,
):
    rows, _ = hidden_ref.shape
    inner = HEADS * HEAD_DIM
    span = SSM_GROUPS * STATE
    per_group = HEADS // SSM_GROUPS
    own_ref[...] = hidden_ref[...]
    values = hidden_ref[...].astype(F32)
    scale = lax.rsqrt(jnp.mean(values * values, axis=-1, keepdims=True) + EPS)
    normed = (values * scale * one_row(gain_ref)).astype(BF16)
    b_part = jnp.dot(normed, b_ref[...], preferred_element_type=F32).astype(BF16)
    c_part = jnp.dot(normed, c_ref[...], preferred_element_type=F32).astype(BF16)
    dt_raw = lax.dot_general(
        normed, dt_ref[...], (((1,), (1,)), ((), ())), preferred_element_type=F32
    ).astype(BF16)
    bc_ref[:, :span] = b_part
    bc_ref[:, span:] = c_part
    taps = taps_ref[...].astype(F32)
    last = taps.shape[0] - 1
    early = one_row(bias_ref)
    for k in range(last):
        early = early + conv_ref[k].astype(F32) * taps[k : k + 1]
    early_ref[...] = jnp.zeros_like(early_ref)
    early_ref[:rows] = early[:, :inner]
    fresh = jnp.concatenate([b_part, c_part], axis=1).astype(F32)
    active = silu(early[:, inner:] + fresh * taps[last:, inner:])
    b_act = active[:, :span]
    c_act = active[:, span:]
    step = jax.nn.softplus(dt_raw.astype(F32) + dt_bias_ref[...])
    decay = jnp.exp(-step * jnp.exp(log_ref[...]))
    coefs = []
    for g in range(SSM_GROUPS):
        cut = slice(g * STATE, (g + 1) * STATE)
        b_wide_ref[g] = jnp.concatenate([b_act[:, cut]] * (LANES // STATE), axis=1)
        c_wide_ref[g] = jnp.concatenate([c_act[:, cut]] * (LANES // STATE), axis=1)
        dots = jnp.sum(b_act[:, cut] * c_act[:, cut], axis=1, keepdims=True)
        coefs.append(jnp.broadcast_to(dots, (rows, per_group)))
    coef = step * jnp.concatenate(coefs, axis=1) + skip_ref[...]
    chan = lax.broadcasted_iota(jnp.int32, (3 * HEADS, inner), 0)
    lane = lax.broadcasted_iota(jnp.int32, (3 * HEADS, inner), 1)
    spread = (lane // HEAD_DIM == chan % HEADS).astype(F32).astype(BF16)
    for values, ref in ((coef, coef_ref), (step, step_ref)):
        parts = jnp.concatenate(three_parts(values), axis=1)
        ref[...] = jnp.zeros_like(ref)
        ref[:rows] = jnp.dot(parts, spread, preferred_element_type=F32)
    for t in range(rows):
        decay_ref[t] = jnp.broadcast_to(to_column(decay[t : t + 1], HEADS), (HEADS, LANES))
    width = share_ref.shape[1]
    split = share_ref.shape[0] // (3 * PAD)
    at = lax.broadcasted_iota(jnp.int32, (rows, width), 1)
    expert = (at // PAD).astype(F32)
    ids = [to_column(ids_ref[k : k + 1].astype(F32), rows) for k in range(TOP)]
    scores = score_ref[...]
    shares = prob_ref[...] * scores / jnp.sum(scores, axis=0, keepdims=True)
    shares = [to_column(shares[k : k + 1], rows) for k in range(TOP)]
    weight = jnp.zeros((rows, width), F32)
    used = jnp.zeros((rows, width), F32)
    numbers = jnp.zeros((rows, LANES), F32)
    lane = lax.broadcasted_iota(jnp.int32, (rows, LANES), 1)
    line = lax.broadcasted_iota(jnp.int32, (rows, LANES), 0)
    for k in range(TOP):
        hit = jnp.broadcast_to(ids[k], (rows, width)) == expert
        weight += jnp.where(hit, jnp.broadcast_to(shares[k], (rows, width)), 0.0)
        used += jnp.where(hit, 1.0, 0.0)
        numbers += jnp.where(lane == k * PAD + line, jnp.broadcast_to(ids[k] + 1.0, (rows, LANES)), 0.0)
    ids_out_ref[...] = jnp.sum(numbers, axis=0, keepdims=True) - 1.0
    seen = jnp.zeros((1, width), F32)
    ranks = []
    for t in range(rows):
        ranks.append(seen)
        seen = seen + used[t : t + 1]
    rank = jnp.concatenate(ranks, axis=0)
    weight = jnp.where(rank == (at % PAD // split).astype(F32), weight, 0.0)
    share_ref[...] = jnp.zeros_like(share_ref)
    for s in range(split):
        cut = jnp.where(at % split == s, weight, 0.0)
        for i, part in enumerate(three_parts(cut)):
            share_ref[(3 * s + i) * PAD : (3 * s + i) * PAD + rows] = part


def read_kernel(
    state_ref, c_ref, decay_ref, keep_ref, out_ref, c_wide_ref, sums_ref, flat_ref, sems
):
    rows, heads, width = state_ref.shape
    lanes = 512

    def copy(chunk):
        cut = pl.ds(pl.multiple_of(chunk * lanes, lanes), lanes)
        return pltpu.make_async_copy(
            state_ref.at[:, :, cut], keep_ref.at[:, :, cut], sems.at[chunk]
        )

    def begin(chunk, carry):
        copy(chunk).start()
        return carry

    lax.fori_loop(0, width // lanes, begin, 0)
    c_wide_ref[...] = widen_rows(c_ref, rows)
    sums_ref[...] = jnp.zeros_like(sums_ref)

    def one(chunk, carry):
        copy(chunk).wait()
        at = pl.multiple_of(chunk * lanes, lanes)
        prods = []
        for k in range(lanes // LANES):
            prod = keep_ref[:, :, pl.ds(at + k * LANES, LANES)] * c_wide_ref[...]
            prods.append(prod.reshape(rows * heads, LANES).astype(BF16))
        lane = lax.broadcasted_iota(jnp.int32, (lanes, HEAD_DIM), 0)
        chan = lax.broadcasted_iota(jnp.int32, (lanes, HEAD_DIM), 1)
        pick = (chunk * (lanes // STATE) + lane // STATE == chan).astype(F32).astype(BF16)
        prods = jnp.concatenate(prods, axis=1)
        sums_ref[...] += jnp.dot(prods, pick, preferred_element_type=F32)
        return carry

    lax.fori_loop(0, width // lanes, one, 0)
    flat_ref[...] = sums_ref[...] * decay_ref[...].reshape(rows * heads, LANES)[:, :HEAD_DIM]
    out_ref[...] = jnp.zeros_like(out_ref)
    for h in range(0, heads, 2):
        pair = [flat_ref[pl.ds(h + j, rows, stride=heads), :] for j in range(2)]
        out_ref[:rows, h * HEAD_DIM : (h + 2) * HEAD_DIM] = jnp.concatenate(pair, axis=1)


def read_state(state_in, c_wide, decay_wide):
    rows, heads, width = state_in.shape
    return call(
        read_kernel,
        (
            jax.ShapeDtypeStruct(state_in.shape, F32),
            jax.ShapeDtypeStruct((PAD, heads * HEAD_DIM), F32),
        ),
        12,
        20_000_000,
        state_in.size * 4,
        in_specs=[pl.BlockSpec(memory_space=pltpu.HBM), vmem(), vmem()],
        out_specs=(vmem(), vmem()),
        scratch_shapes=[
            pltpu.VMEM((rows, heads, LANES), F32),
            pltpu.VMEM((rows * heads, HEAD_DIM), F32),
            pltpu.VMEM((rows * heads, HEAD_DIM), F32),
            pltpu.SemaphoreType.DMA((width // 512,)),
        ],
        name="read_state",
    )(state_in, c_wide, decay_wide)


def write_kernel(
    state_ref, xs_ref, b_ref, decay_ref, conv_ref, fresh_ref, bc_ref,
    out_ref, conv_out_ref, parts_ref, b_wide_ref, new_ref, sems,
):
    rows, heads, width = state_ref.shape
    lanes = 512
    inner = heads * HEAD_DIM
    for h in range(heads):
        parts_ref[pl.ds(h, rows, stride=heads), :] = xs_ref[
            :rows, h * HEAD_DIM : (h + 1) * HEAD_DIM
        ]
    parts = jnp.concatenate(three_parts(parts_ref[...]), axis=1)
    b_wide_ref[...] = widen_rows(b_ref, rows)

    def copy(chunk):
        cut = pl.ds(pl.multiple_of(chunk * lanes, lanes), lanes)
        return pltpu.make_async_copy(
            new_ref.at[:, :, cut], out_ref.at[:, :, cut], sems.at[chunk]
        )

    def one(chunk, carry):
        at = pl.multiple_of(chunk * lanes, lanes)
        lane = lax.broadcasted_iota(jnp.int32, (3 * HEAD_DIM, lanes), 1)
        chan = lax.broadcasted_iota(jnp.int32, (3 * HEAD_DIM, lanes), 0)
        spread = chunk * (lanes // STATE) + lane // STATE == chan % HEAD_DIM
        wide = jnp.dot(parts, spread.astype(F32).astype(BF16), preferred_element_type=F32)
        wide = wide.reshape(rows, heads, lanes)
        for k in range(lanes // LANES):
            cut = pl.ds(at + k * LANES, LANES)
            new_ref[:, :, cut] = (
                decay_ref[...] * state_ref[:, :, cut]
                + wide[:, :, k * LANES : (k + 1) * LANES] * b_wide_ref[...]
            )
        copy(chunk).start()
        return carry

    lax.fori_loop(0, width // lanes, one, 0)
    taps = conv_ref.shape[0]
    for k in range(1, taps):
        conv_out_ref[k - 1] = conv_ref[k]
    conv_out_ref[taps - 1, :, :inner] = fresh_ref[:rows]
    conv_out_ref[taps - 1, :, inner:] = bc_ref[...]

    def done(chunk, carry):
        copy(chunk).wait()
        return carry

    lax.fori_loop(0, width // lanes, done, 0)


def write_state(state, xs, b_wide, decay_wide, conv, fresh, bc):
    rows, heads, width = state.shape
    return call(
        write_kernel,
        (jax.ShapeDtypeStruct(state.shape, F32), jax.ShapeDtypeStruct(conv.shape, BF16)),
        16,
        40_000_000,
        state.size * 4,
        in_specs=[vmem()] * 7,
        out_specs=(pl.BlockSpec(memory_space=pltpu.HBM), vmem()),
        scratch_shapes=[
            pltpu.VMEM((rows * heads, HEAD_DIM), F32),
            pltpu.VMEM((rows, heads, LANES), F32),
            pltpu.VMEM(state.shape, F32),
            pltpu.SemaphoreType.DMA((width // 512,)),
        ],
        name="write_state",
    )(state, xs, b_wide, decay_wide, conv, fresh, bc)


def project_kernel(*refs):
    *parts, z_ref, x_ref, gain_ref, ids_ref, out_ref, rows_ref = refs
    me = lax.axis_index("ep")
    count = rows_ref.shape[0]
    rows, model_width = parts[0].shape[1:]
    cols = z_ref.shape[1]
    rows_ref[:, rows:, :] = jnp.zeros((count, PAD - rows, model_width), BF16)
    for part, k, owner in owners(me, parts, count, AHEAD["first"]):
        rows_ref[owner, :rows] = part[k]
    values = rows_ref[...].astype(F32).reshape(count * PAD, model_width)
    scale = lax.rsqrt(jnp.mean(values * values, axis=-1, keepdims=True) + EPS)
    normed = (values * scale * one_row(gain_ref)).astype(BF16)
    z_cols = jnp.dot(normed, z_ref[...], preferred_element_type=F32)
    x_cols = jnp.dot(normed, x_ref[...], preferred_element_type=F32).astype(BF16)
    spare = lax.broadcasted_iota(jnp.int32, (count * PAD, LANES), 0) % PAD == rows
    ids = jnp.broadcast_to(ids_ref[...], (count * PAD, LANES))
    first = jnp.where(spare, ids, z_cols[:, :LANES])
    z_cols = jnp.concatenate([first, z_cols[:, LANES:]], axis=1) if cols > LANES else first
    out_ref[:, :, :cols] = z_cols.astype(BF16).reshape(count, PAD, cols)
    out_ref[:, :, cols:] = x_cols.reshape(count, PAD, cols)


def gate_kernel(
    zx_ref, early_ref, taps_ref, coef_ref, read_ref, step_ref, gain_ref, y_ref, xs_ref, fresh_ref
):
    count, _, both = zx_ref.shape
    cols = both // 2
    inner = count * cols
    z = jnp.concatenate([zx_ref[j, :, :cols] for j in range(count)], axis=1)
    x = jnp.concatenate([zx_ref[j, :, cols:] for j in range(count)], axis=1)
    fresh_ref[...] = x
    last = taps_ref.shape[0] - 1
    tap = taps_ref[...].astype(F32)[last:, :inner]
    x_act = silu(early_ref[...] + x.astype(F32) * tap)
    xs_ref[...] = step_ref[...] * x_act
    gated = (read_ref[...] + coef_ref[...] * x_act) * silu(z.astype(F32))
    scale = lax.rsqrt(jnp.mean(gated * gated, axis=-1, keepdims=True) + EPS)
    y_ref[...] = (gated * scale * one_row(gain_ref)).astype(BF16)


def output_kernel(*refs):
    *parts, weight_ref, pick_ref, out_ref, cols_ref = refs
    count, slots, col = out_ref.shape
    width = weight_ref.shape[0]
    rows = jnp.concatenate(
        [part[...].reshape(part.shape[0] * PAD, width) for part in parts], axis=0
    )
    cols = jnp.dot(rows, weight_ref[...], preferred_element_type=F32)
    blocks = owners(lax.axis_index("ep"), parts, count, AHEAD["second"])
    for i, (_, _, owner) in enumerate(blocks):
        cols_ref[owner] = cols[i * PAD : (i + 1) * PAD]
    cols = cols_ref[...].reshape(count * PAD, col).astype(BF16)
    pick = pick_ref[...].reshape(count * slots, count * PAD)
    picked = jnp.dot(pick, cols, preferred_element_type=F32)
    out_ref[...] = picked.astype(BF16).reshape(count, slots, col)


def choose_kernel(zx_ref, rows_ref, pick_ref, hidden_ref, capacity, rows):
    count, slots, tokens = pick_ref.shape
    ids = jnp.concatenate(
        [zx_ref[j, :, :LANES].astype(F32)[rows : rows + 1] for j in range(count)], axis=0
    ).astype(BF16)
    source = lax.broadcasted_iota(jnp.int32, (LANES, tokens), 0)
    lane = lax.broadcasted_iota(jnp.int32, (LANES, tokens), 1)
    mine = lax.broadcasted_iota(jnp.int32, (count, tokens), 0)
    token = lax.broadcasted_iota(jnp.int32, (count, tokens), 1)
    named = jnp.zeros((count, tokens), F32)
    for k in range(TOP):
        take = (source == k * PAD + lane % PAD).astype(F32).astype(BF16)
        wide = jnp.dot(ids, take, preferred_element_type=F32)
        line = jnp.sum(jnp.where(mine == token // PAD, wide, 0.0), axis=0, keepdims=True)
        named += (jnp.broadcast_to(line, (count, tokens)) == mine.astype(F32)).astype(F32)
    row = lax.broadcasted_iota(jnp.int32, (tokens, tokens), 0)
    col = lax.broadcasted_iota(jnp.int32, (tokens, tokens), 1)
    before = ((row // PAD == col // PAD) & (row < col)).astype(F32).astype(BF16)
    place = jnp.dot(named.astype(BF16), before, preferred_element_type=F32)
    place = jnp.where(named > 0.5, place, -1.0)
    slot = lax.broadcasted_iota(jnp.int32, (slots, tokens), 0)
    lane = lax.broadcasted_iota(jnp.int32, (slots, tokens), 1)
    taken = slots - PAD
    from_sender = (slot // capacity == lane // PAD) & (slot < taken)
    wanted = jnp.where(from_sender, (slot % capacity).astype(F32), -2.0)
    for j in range(count):
        hit = wanted == jnp.broadcast_to(place[j : j + 1], (slots, tokens))
        own = lane - j * PAD == slot - taken
        pick_ref[j] = ((hit | (own & (slot >= taken)))).astype(F32).astype(BF16)
    mine = pick_ref[lax.axis_index("ep")]
    hidden = rows_ref[...].reshape(tokens, rows_ref.shape[2])
    hidden_ref[...] = jnp.dot(mine, hidden, preferred_element_type=F32).astype(BF16)


def expert_kernel(
    hidden_ref, cols_ref, gain_ref, gate_ref, up_ref, down_ref, out_ref, mixed_ref, capacity
):
    count, slots, _ = cols_ref.shape
    model_width = hidden_ref.shape[1]
    projected = jnp.concatenate([cols_ref[j] for j in range(count)], axis=1)
    mixed = (hidden_ref[...].astype(F32) + projected.astype(F32)).astype(BF16)
    mixed_ref[...] = mixed[slots - PAD :]
    wide = mixed.astype(F32)
    scale = lax.rsqrt(jnp.mean(wide * wide, axis=-1, keepdims=True) + EPS)
    normed = (wide * scale * one_row(gain_ref)).astype(BF16)
    gate = jnp.dot(normed, gate_ref[0], preferred_element_type=F32)
    up = jnp.dot(normed, up_ref[0], preferred_element_type=F32)
    act = (silu(gate) * up).astype(BF16)
    width = out_ref.shape[2]
    split = model_width // width
    tokens = count * PAD
    row = lax.broadcasted_iota(jnp.int32, (tokens, slots), 0)
    slot = lax.broadcasted_iota(jnp.int32, (tokens, slots), 1)
    place = row % PAD // split
    spread = (slot == row // PAD * capacity + place) & (place < capacity)
    act = jnp.dot(spread.astype(F32).astype(BF16), act, preferred_element_type=F32).astype(BF16)
    result = jnp.dot(act, down_ref[0], preferred_element_type=F32)
    row = lax.broadcasted_iota(jnp.int32, (tokens, width), 0) % split
    folded = result[:, :width]
    for s in range(1, split):
        folded = jnp.where(row == s, result[:, s * width : (s + 1) * width], folded)
    out_ref[...] = folded.astype(BF16).reshape(count, PAD, width)


def combine_kernel(back_ref, share_ref, mixed_ref, out_ref):
    count, _, width = back_ref.shape
    rows, model_width = out_ref.shape
    values = back_ref[...].reshape(count * PAD, width)
    sums = jnp.dot(share_ref[...], values, preferred_element_type=F32)
    for s in range(model_width // width):
        at = 3 * PAD * s
        total = sums[at : at + PAD] + sums[at + PAD : at + 2 * PAD] + sums[at + 2 * PAD : at + 3 * PAD]
        cut = slice(s * width, (s + 1) * width)
        out_ref[:, cut] = (mixed_ref[:, cut].astype(F32) + total)[:rows].astype(BF16)


def body(
    hidden,
    state_in,
    conv_state,
    expert_ids,
    group_prob,
    expert_score,
    first_gain,
    z_weight,
    x_weight,
    b_weight,
    c_weight,
    dt_weight,
    conv_weight,
    conv_bias,
    dt_bias,
    decay_log,
    skip_gain,
    inner_gain,
    out_weight,
    second_gain,
    expert_gate,
    expert_up,
    expert_down,
):
    rows, model_width = hidden.shape
    inner = HEADS * HEAD_DIM
    span = SSM_GROUPS * STATE
    count = lax.axis_size("ep")
    tokens = count * PAD
    capacity = max(2, (3 * rows * TOP + 2 * count - 1) // (2 * count))
    slots = 2
    while slots < capacity:
        slots *= 2
    split = PAD // slots

    def streamed(array):
        return pltpu.with_memory_space_constraint(array, pltpu.HBM)

    conv_state = conv_state.transpose(1, 0, 2)

    def lines(vector):
        return vector.reshape(-1, LANES)


    def wide(kind):
        return jax.ShapeDtypeStruct((PAD, inner), kind)

    early, coef, step, b_wide, c_wide, decay_wide, bc, ids_row, share_rows, own = call(
        local_kernel,
        (
            wide(F32),
            wide(F32),
            wide(F32),
            jax.ShapeDtypeStruct((SSM_GROUPS, rows, LANES), F32),
            jax.ShapeDtypeStruct((SSM_GROUPS, rows, LANES), F32),
            jax.ShapeDtypeStruct((rows, HEADS, LANES), F32),
            jax.ShapeDtypeStruct((rows, 2 * span), BF16),
            jax.ShapeDtypeStruct((1, LANES), F32),
            jax.ShapeDtypeStruct((split * 3 * PAD, tokens), BF16),
            jax.ShapeDtypeStruct(hidden.shape, BF16),
        ),
        16,
        10_000_000,
        4_000_000,
        in_specs=[vmem()] * 14,
        out_specs=(vmem(),) * 10,
        name="local",
    )(
        *[
            streamed(array)
            for array in (
                hidden,
                lines(first_gain),
                b_weight,
                c_weight,
                dt_weight.T,
                conv_state,
                conv_weight,
                lines(conv_bias),
                dt_bias[None, :],
                decay_log[None, :],
                skip_gain[None, :],
                expert_ids.T,
                group_prob[None, :],
                expert_score.T,
            )
        ]
    )
    parts = gather(hidden, count, AHEAD["first"], own)
    state, read = read_state(streamed(state_in), c_wide, decay_wide)

    cols = z_weight.shape[1]
    zx, all_rows = call(
        project_kernel,
        (
            jax.ShapeDtypeStruct((count, PAD, 2 * cols), BF16),
            jax.ShapeDtypeStruct((count, PAD, model_width), BF16),
        ),
        12,
        4 * tokens * model_width * cols,
        4 * model_width * cols,
        in_specs=[vmem()] * 8,
        out_specs=(vmem(), vmem()),
        name="project",
    )(*parts, z_weight, x_weight, lines(first_gain), ids_row)
    zx = lax.all_to_all(zx, "ep", split_axis=0, concat_axis=0, tiled=True)
    y_mix, xs, x_fresh = call(
        gate_kernel,
        (wide(BF16), wide(F32), wide(BF16)),
        8,
        40 * PAD * inner,
        30 * PAD * inner,
        in_specs=[vmem()] * 7,
        out_specs=(vmem(),) * 3,
        name="gate",
    )(zx, early, conv_weight, coef, read, step, lines(inner_gain))

    taken = count * capacity + PAD
    pick, chosen = call(
        functools.partial(choose_kernel, capacity=capacity, rows=rows),
        (
            jax.ShapeDtypeStruct((count, taken, tokens), BF16),
            jax.ShapeDtypeStruct((taken, model_width), BF16),
        ),
        8,
        2 * taken * tokens * model_width,
        2 * tokens * model_width,
        in_specs=[vmem()] * 2,
        out_specs=(vmem(), vmem()),
        name="choose",
    )(zx, all_rows)

    parts = gather(y_mix, count, AHEAD["second"])
    state_out, conv_out = write_state(
        state, xs, b_wide, decay_wide, conv_state, x_fresh, bc
    )
    out_cols = out_weight.shape[1]
    slab = call(
        output_kernel,
        jax.ShapeDtypeStruct((count, taken, out_cols), BF16),
        12,
        2 * tokens * inner * out_cols,
        2 * inner * out_cols,
        in_specs=[vmem()] * 6,
        out_specs=vmem(),
        scratch_shapes=[pltpu.VMEM((count, PAD, out_cols), F32)],
        name="output",
    )(*parts, out_weight, pick)

    slab = lax.all_to_all(slab, "ep", split_axis=0, concat_axis=0, tiled=True)
    back, mixed = call(
        functools.partial(expert_kernel, capacity=capacity),
        (
            jax.ShapeDtypeStruct((count, PAD, model_width // split), BF16),
            jax.ShapeDtypeStruct((PAD, model_width), BF16),
        ),
        24,
        6 * tokens * expert_gate.shape[1] * expert_gate.shape[2],
        6 * expert_gate.shape[1] * expert_gate.shape[2],
        in_specs=[vmem()] * 6,
        out_specs=(vmem(), vmem()),
        name="expert",
    )(chosen, slab, lines(second_gain), expert_gate, expert_up, expert_down)

    back = lax.all_to_all(back, "ep", split_axis=0, concat_axis=0, tiled=True)
    layer_out = call(
        combine_kernel,
        jax.ShapeDtypeStruct((rows, model_width), BF16),
        8,
        2 * 6 * PAD * tokens * model_width,
        2 * tokens * model_width,
        in_specs=[vmem()] * 3,
        out_specs=vmem(),
        name="combine",
    )(back, share_rows, mixed)
    return layer_out, state_out, conv_out.transpose(1, 0, 2)


def solution(mesh):
    seq = ("grp", "ep")
    in_specs = (
        P(seq, None),
        P(seq, None, None),
        P(seq, None, None),
        P(seq, None),
        P(seq),
        P(seq, None),
        P(),
        P(None, "ep"),
        P(None, "ep"),
        P(),
        P(),
        P(),
        P(),
        P(),
        P(),
        P(),
        P(),
        P(),
        P(None, "ep"),
        P(),
        P("ep", None, None),
        P("ep", None, None),
        P("ep", None, None),
    )
    out_specs = (P(seq, None), P(seq, None, None), P(seq, None, None))

    return jax.shard_map(body, mesh=mesh, in_specs=in_specs, out_specs=out_specs, check_vma=False)
```

profile of v0, /device:TPU:0, one launch (start us, length us, event | category | flops | bytes accessed | tf_op | source)
XLA Modules:
  0.0 98.2 jit_solution(495965097964685462)
XLA Ops:
  0.6 5.1 %collective-permute-start = (bf16[7,2048]{1,0:T(8,128)(2,1)}, bf16[7,2048]{1,0:T(8,128)(2,1)S(1)}, u32[]{:S(2)}, u32[]{:S(2)}) collective-permute-start(bf16[7,2048]{1,0:T(8,128)(2,1)} %hidden_ref.1), channel_id=1, source_target_pairs={{0,12},{1,13},{2,14},{3,15},{4,8},{5,9},{6,10},{7,11},{8,4},{9,5},... | collective-permute-start | bytes 86024 | tf_op jit(solution)/shard_map/ppermute | solution.py:42
  6.4 3.1 %local.1 = (f32[8,4096]{1,0:T(8,128)S(1)}, f32[8,4096]{1,0:T(8,128)S(1)}, f32[8,4096]{1,0:T(8,128)S(1)}, f32[4,7,128]{2,1,0:T(8,128)S(1)}, f32[4,7,128]{2,1,0:T(...) custom-call(bf16[7,2048]{1,0:T(8,128)(2,1)} %hidden_ref.1, ...), custom_call_target="tpu_custom_call" | custom-call | flops 10000000 | bytes 4000000 | tf_op jit(solution)/shard_map/local/pallas_call | solution.py:522
  12.1 1.7 %collective-permute-start.3 = (bf16[4,7,2048]{2,1,0:T(8,128)(2,1)S(1)}, bf16[4,7,2048]{2,1,0:T(8,128)(2,1)S(1)}, u32[]{:S(2)}, u32[]{:S(2)}) collective-permute-start(bf16[4,7,2048]{2,1,0:T(8,128)(2,1)S(1)} %join.3.refs_0_), channel_id=1, source_target_pairs={{0,2},{1,3},{2,0},{3,1},{4,6},{5,7},{6,4},{7,5},{8,10},{9,11},{10,... | collective-permute-start | bytes 344072 | tf_op jit(solution)/shard_map/ppermute | solution.py:42
  13.8 3.3 %collective-permute-done.3.refs_1_ = bf16[4,7,2048]{2,1,0:T(8,128)(2,1)S(1)} collective-permute-done((bf16[4,7,2048]{2,1,0:T(8,128)(2,1)S(1)}, bf16[4,7,2048]{2,1,0:T(8,128)(2,1)S(1)}, u32[]{:S(2)}, u32[]{:S(2)}) %collective-permute-start.3) | collective-permute-done | bytes 114720 | tf_op jit(solution)/shard_map/ppermute | solution.py:42
  17.1 1.3 %collective-permute-done.5.refs_3_ = bf16[4,7,2048]{2,1,0:T(8,128)(2,1)S(1)} collective-permute-done((bf16[4,7,2048]{2,1,0:T(8,128)(2,1)S(1)}, bf16[4,7,2048]{2,1,0:T(8,128)(2,1)S(1)}, u32[]{:S(2)}, u32[]{:S(2)}) %collective-permute-start.5) | collective-permute-done | bytes 114720 | tf_op jit(solution)/shard_map/ppermute | solution.py:42
  18.5 1.2 %copy-done.5 = bf16[2048,256]{1,0:T(8,128)(2,1)S(1)} copy-done((bf16[2048,256]{1,0:T(8,128)(2,1)S(1)}, bf16[2048,256]{1,0:T(8,128)(2,1)}, u32[]{:S(2)}) %copy-start.5) | copy-done | bytes 1048600
  19.7 1.2 %copy-done.6 = bf16[2048,256]{1,0:T(8,128)(2,1)S(1)} copy-done((bf16[2048,256]{1,0:T(8,128)(2,1)S(1)}, bf16[2048,256]{1,0:T(8,128)(2,1)}, u32[]{:S(2)}) %copy-start.6) | copy-done | bytes 1048600
  22.3 0.8 copy-done.9
  23.8 6.1 %all-to-all-start = ((bf16[16,8,512]{2,1,0:T(8,128)(2,1)}), bf16[16,8,512]{2,1,0:T(8,128)(2,1)S(1)}, u32[]{:S(2)}, u32[]{:S(2)}) async-start(bf16[16,8,512]{2,1,0:T(8,128)(2,1)} %copy-done.14), calls=%async_computation | async-start | bytes 262144 | tf_op jit(solution)/shard_map/all_to_all | solution.py:580
  30.6 3.9 %read_state.1 = (f32[7,64,4096]{2,1,0:T(8,128)S(1)}, f32[8,4096]{1,0:T(8,128)S(1)}) custom-call(f32[7,64,4096]{2,1,0:T(8,128)} %state_ref.1, f32[4,7,128]{2,1,0:T(8,128)S(1)} %copy-done.28, f32[7,64,128]{2,1,0:T(8,128)S(1)} %get-tuple-element.34.decay_ref), custom_call_target="tpu_custom_call" | custom-call | flops 20000000 | bytes 7340032 | tf_op jit(solution)/shard_map/read_state/pallas_call | solution.py:250
  34.5 3.0 %copy-done = f32[7,64,4096]{2,1,0:T(8,128)} copy-done((f32[7,64,4096]{2,1,0:T(8,128)}, f32[7,64,4096]{2,1,0:T(8,128)S(1)}, u32[]{:S(2)}) %copy-start) | copy-done | bytes 7340056
  38.2 0.9 copy-done.16
  39.1 0.9 copy-done.18
  40.0 0.9 copy-done.20
  40.9 0.9 copy-done.22
  42.7 3.8 %collective-permute-start.6 = (bf16[8,4096]{1,0:T(8,128)(2,1)S(1)}, bf16[8,4096]{1,0:T(8,128)(2,1)S(1)}, u32[]{:S(2)}, u32[]{:S(2)}) collective-permute-start(bf16[8,4096]{1,0:T(8,128)(2,1)S(1)} %get-tuple-element.37.refs_0_), channel_id=1, source_target_pairs={{0,12},{1,13},{2,14},{3,15},{4,8},{5,9},{6,10},{7,11},{8,4},{9,5},... | collective-permute-start | bytes 196616 | tf_op jit(solution)/shard_map/ppermute | solution.py:42
  47.2 1.9 %collective-permute-start.9 = (bf16[8,4096]{1,0:T(8,128)(2,1)S(1)}, bf16[8,4096]{1,0:T(8,128)(2,1)S(1)}, u32[]{:S(2)}, u32[]{:S(2)}) collective-permute-start(bf16[8,4096]{1,0:T(8,128)(2,1)S(1)} %get-tuple-element.37.refs_0_), channel_id=1, source_target_pairs={{0,2},{1,3},{2,0},{3,1},{4,6},{5,7},{6,4},{7,5},{8,10},{9,11},{10,... | collective-permute-start | bytes 196616 | tf_op jit(solution)/shard_map/ppermute | solution.py:42
  49.1 2.0 %collective-permute-start.10 = (bf16[8,4096]{1,0:T(8,128)(2,1)S(1)}, bf16[8,4096]{1,0:T(8,128)(2,1)S(1)}, u32[]{:S(2)}, u32[]{:S(2)}) collective-permute-start(bf16[8,4096]{1,0:T(8,128)(2,1)S(1)} %collective-permute-done.6.refs_1_), channel_id=1, source_target_pairs={{0,2},{1,3},{2,0},{3,1},{4,6},{5,7},{6,4},{7,5},{8,10},{9,11},{10,... | collective-permute-start | bytes 196616 | tf_op jit(solution)/shard_map/ppermute | solution.py:42
  51.1 1.4 %collective-permute-done.7.refs_2_.refs_0_ = bf16[8,4096]{1,0:T(8,128)(2,1)S(1)} collective-permute-done((bf16[8,4096]{1,0:T(8,128)(2,1)S(1)}, bf16[8,4096]{1,0:T(8,128)(2,1)S(1)}, u32[]{:S(2)}, u32[]{:S(2)}) %collective-permute-start.7) | collective-permute-done | bytes 65568 | tf_op jit(solution)/shard_map/ppermute | solution.py:42
  52.5 0.9 collective-permute-done.10.refs_5_
  53.5 2.1 %collective-permute-start.11 = (bf16[2,8,4096]{2,1,0:T(8,128)(2,1)S(1)}, bf16[2,8,4096]{2,1,0:T(8,128)(2,1)S(1)}, u32[]{:S(2)}, u32[]{:S(2)}) collective-permute-start(bf16[2,8,4096]{2,1,0:T(8,128)(2,1)S(1)} %join.5), channel_id=1, source_target_pairs={{0,2},{1,3},{2,0},{3,1},{4,6},{5,7},{6,4},{7,5},{8,10},{9,11},{10,... | collective-permute-start | bytes 393224 | tf_op jit(solution)/shard_map/ppermute | solution.py:42
  55.6 4.2 %collective-permute-done.11.refs_1_ = bf16[2,8,4096]{2,1,0:T(8,128)(2,1)S(1)} collective-permute-done((bf16[2,8,4096]{2,1,0:T(8,128)(2,1)S(1)}, bf16[2,8,4096]{2,1,0:T(8,128)(2,1)S(1)}, u32[]{:S(2)}, u32[]{:S(2)}) %collective-permute-start.11) | collective-permute-done | bytes 131104 | tf_op jit(solution)/shard_map/ppermute | solution.py:42
  59.8 1.0 %copy-done.10 = bf16[16,8,2048]{2,1,0:T(8,128)(2,1)S(1)} copy-done((bf16[16,8,2048]{2,1,0:T(8,128)(2,1)S(1)}, bf16[16,8,2048]{2,1,0:T(8,128)(2,1)}, u32[]{:S(2)}) %copy-start.10) | copy-done | bytes 524312
  62.1 15.7 %all_to_all.15.cols_ref = bf16[16,56,128]{2,1,0:T(8,128)(2,1)S(1)} all-to-all(bf16[16,56,128]{2,1,0:T(8,128)(2,1)S(1)} %output.1), channel_id=1, replica_groups=mesh['grp'=2,'ep'=16] {'ep'}, dimensions={0} | all-to-all | bytes 458752 | tf_op jit(solution)/shard_map/all_to_all | solution.py:624
  77.8 1.6 %copy-done.3 = bf16[1,2048,512]{2,1,0:T(8,128)(2,1)S(1)} copy-done((bf16[1,2048,512]{2,1,0:T(8,128)(2,1)S(1)}, bf16[1,2048,512]{2,1,0:T(8,128)(2,1)}, u32[]{:S(2)}) %copy-start.3) | copy-done | bytes 2097176
  79.4 1.6 %copy-done.4 = bf16[1,512,2048]{2,1,0:T(8,128)(2,1)S(1)} copy-done((bf16[1,512,2048]{2,1,0:T(8,128)(2,1)S(1)}, bf16[1,512,2048]{2,1,0:T(8,128)(2,1)}, u32[]{:S(2)}) %copy-start.4) | copy-done | bytes 2097176
  81.7 2.2 %expert.1 = (bf16[16,8,1024]{2,1,0:T(8,128)(2,1)}, bf16[8,2048]{1,0:T(8,128)(2,1)S(1)}) custom-call(bf16[56,2048]{1,0:T(8,128)(2,1)S(1)} %get-tuple-element.30.hidden_ref, bf16[16,56,128]{2,1,0:T(8,128)(2,1)S(1)} %all_to_all.15.cols_ref, bf16[16,128]{1,0:T(8,128)(2,1)S(1)} %bitcast.18, bf16[1,2048,512]{2,1,0:T(8,128)(2,1)S(1)} %copy-done.2, ...), custom_call_target="tpu_custom_call" | custom-call | flops 805306368 | bytes 6291456 | tf_op jit(solution)/shard_map/expert/pallas_call | solution.py:625
  83.9 3.5 %all-to-all-start.2 = ((bf16[16,8,1024]{2,1,0:T(8,128)(2,1)}), bf16[16,8,1024]{2,1,0:T(8,128)(2,1)S(1)}, u32[]{:S(2)}, u32[]{:S(2)}) async-start(bf16[16,8,1024]{2,1,0:T(8,128)(2,1)} %get-tuple-element.39), calls=%async_computation.2 | async-start | bytes 524288 | tf_op jit(solution)/shard_map/all_to_all | solution.py:639
  87.5 3.1 %copy-done.1 = f32[7,64,4096]{2,1,0:T(8,128)S(1)} copy-done((f32[7,64,4096]{2,1,0:T(8,128)S(1)}, f32[7,64,4096]{2,1,0:T(8,128)}, u32[]{:S(2)}) %copy-start.1) | copy-done | bytes 7340056
  90.6 5.0 %write_state.1 = (f32[7,64,4096]{2,1,0:T(8,128)}, bf16[3,7,4608]{2,1,0:T(8,128)(2,1)}) custom-call(f32[7,64,4096]{2,1,0:T(8,128)S(1)} %copy-done.1, f32[8,4096]{1,0:T(8,128)S(1)} %copy-done.13, f32[4,7,128]{2,1,0:T(8,128)S(1)} %copy-done.26, f32[7,64,128]{2,1,0:T(8,128)S(1)} %get-tuple-element.34.decay_ref, bf16[3,7,4608]{2,1,0:T(8,128)(2,1)S(1)} %bitcast.14, ...), custom_call_target="tpu_custom_call" | custom-call | flops 40000000 | bytes 7340032 | tf_op jit(solution)/shard_map/write_state/pallas_call | solution.py:323
  95.6 1.8 %all-to-all-done.2.back_ref = bf16[16,8,1024]{2,1,0:T(8,128)(2,1)S(1)} async-done(((bf16[16,8,1024]{2,1,0:T(8,128)(2,1)}), bf16[16,8,1024]{2,1,0:T(8,128)(2,1)S(1)}, u32[]{:S(2)}, u32[]{:S(2)}) %all-to-all-start.2) | async-done | bytes 262176 | tf_op jit(solution)/shard_map/all_to_all | solution.py:639
  97.4 0.8 combine.1
  (81 shorter events, 10.2 us)
Async XLA Ops:
  0.6 37.5 %copy-start.11 = (bf16[4,4608]{1,0:T(4,128)(2,1)S(1)}, bf16[4,4608]{1,0:T(4,128)(2,1)}, u32[]{:S(2)}) copy-start(bf16[4,4608]{1,0:T(4,128)(2,1)} %taps_ref.3) | copy-start | bytes 110596
  0.6 11.4 %collective-permute-start = (bf16[7,2048]{1,0:T(8,128)(2,1)}, bf16[7,2048]{1,0:T(8,128)(2,1)S(1)}, u32[]{:S(2)}, u32[]{:S(2)}) collective-permute-start(bf16[7,2048]{1,0:T(8,128)(2,1)} %hidden_ref.1), channel_id=1, source_target_pairs={{0,12},{1,13},{2,14},{3,15},{4,8},{5,9},{6,10},{7,11},{8,4},{9,5},... | collective-permute-start | bytes 86024 | tf_op jit(solution)/shard_map/ppermute | solution.py:42
  5.8 6.3 %collective-permute-start.1 = (bf16[7,2048]{1,0:T(8,128)(2,1)}, bf16[7,2048]{1,0:T(8,128)(2,1)S(1)}, u32[]{:S(2)}, u32[]{:S(2)}) collective-permute-start(bf16[7,2048]{1,0:T(8,128)(2,1)} %hidden_ref.1), channel_id=1, source_target_pairs={{0,8},{1,9},{2,10},{3,11},{4,12},{5,13},{6,14},{7,15},{8,0},{9,1},... | collective-permute-start | bytes 86024 | tf_op jit(solution)/shard_map/ppermute | solution.py:42
  5.8 6.3 %collective-permute-start.2 = (bf16[7,2048]{1,0:T(8,128)(2,1)}, bf16[7,2048]{1,0:T(8,128)(2,1)S(1)}, u32[]{:S(2)}, u32[]{:S(2)}) collective-permute-start(bf16[7,2048]{1,0:T(8,128)(2,1)} %hidden_ref.1), channel_id=1, source_target_pairs={{0,4},{1,5},{2,6},{3,7},{4,0},{5,1},{6,2},{7,3},{8,12},{9,13},{10,... | collective-permute-start | bytes 86024 | tf_op jit(solution)/shard_map/ppermute | solution.py:42
  6.4 54.9 %copy-start.7 = (bf16[4096,128]{1,0:T(8,128)(2,1)S(1)}, bf16[4096,128]{1,0:T(8,128)(2,1)}, u32[]{:S(2)}) copy-start(bf16[4096,128]{1,0:T(8,128)(2,1)} %refs_4_.3) | copy-start | bytes 3145732
  12.0 6.4 %copy-start.17 = (f32[8,4096]{1,0:T(8,128)}, f32[8,4096]{1,0:T(8,128)S(1)}, u32[]{:S(2)}) copy-start(f32[8,4096]{1,0:T(8,128)S(1)} %get-tuple-element.32.coef_ref) | copy-start | bytes 393220
  12.0 6.4 %copy-start.19 = (f32[8,4096]{1,0:T(8,128)}, f32[8,4096]{1,0:T(8,128)S(1)}, u32[]{:S(2)}) copy-start(f32[8,4096]{1,0:T(8,128)S(1)} %get-tuple-element.36.step_ref) | copy-start | bytes 393220
  12.1 5.0 %collective-permute-start.3 = (bf16[4,7,2048]{2,1,0:T(8,128)(2,1)S(1)}, bf16[4,7,2048]{2,1,0:T(8,128)(2,1)S(1)}, u32[]{:S(2)}, u32[]{:S(2)}) collective-permute-start(bf16[4,7,2048]{2,1,0:T(8,128)(2,1)S(1)} %join.3.refs_0_), channel_id=1, source_target_pairs={{0,2},{1,3},{2,0},{3,1},{4,6},{5,7},{6,4},{7,5},{8,10},{9,11},{10,... | collective-permute-start | bytes 344072 | tf_op jit(solution)/shard_map/ppermute | solution.py:42
  13.8 3.3 %collective-permute-start.4 = (bf16[4,7,2048]{2,1,0:T(8,128)(2,1)S(1)}, bf16[4,7,2048]{2,1,0:T(8,128)(2,1)S(1)}, u32[]{:S(2)}, u32[]{:S(2)}) collective-permute-start(bf16[4,7,2048]{2,1,0:T(8,128)(2,1)S(1)} %join.3.refs_0_), channel_id=1, source_target_pairs={{0,1},{1,0},{2,3},{3,2},{4,5},{5,4},{6,7},{7,6},{8,9},{9,8},{10,11... | collective-permute-start | bytes 344072 | tf_op jit(solution)/shard_map/ppermute | solution.py:42
  17.1 1.3 %collective-permute-start.5 = (bf16[4,7,2048]{2,1,0:T(8,128)(2,1)S(1)}, bf16[4,7,2048]{2,1,0:T(8,128)(2,1)S(1)}, u32[]{:S(2)}, u32[]{:S(2)}) collective-permute-start(bf16[4,7,2048]{2,1,0:T(8,128)(2,1)S(1)} %collective-permute-done.3.refs_1_), channel_id=1, source_target_pairs={{0,1},{1,0},{2,3},{3,2},{4,5},{5,4},{6,7},{7,6},{8,9},{9,8},{10,11... | collective-permute-start | bytes 344072 | tf_op jit(solution)/shard_map/ppermute | solution.py:42
  21.6 56.2 %copy-start.2 = (bf16[1,2048,512]{2,1,0:T(8,128)(2,1)S(1)}, bf16[1,2048,512]{2,1,0:T(8,128)(2,1)}, u32[]{:S(2)}) copy-start(bf16[1,2048,512]{2,1,0:T(8,128)(2,1)} %gate_ref.1) | copy-start | bytes 6291460
  23.8 14.4 %all-to-all-start = ((bf16[16,8,512]{2,1,0:T(8,128)(2,1)}), bf16[16,8,512]{2,1,0:T(8,128)(2,1)S(1)}, u32[]{:S(2)}, u32[]{:S(2)}) async-start(bf16[16,8,512]{2,1,0:T(8,128)(2,1)} %copy-done.14), calls=%async_computation | async-start | bytes 262144 | tf_op jit(solution)/shard_map/all_to_all | solution.py:580
  34.5 3.1 %copy-start = (f32[7,64,4096]{2,1,0:T(8,128)}, f32[7,64,4096]{2,1,0:T(8,128)S(1)}, u32[]{:S(2)}) copy-start(f32[7,64,4096]{2,1,0:T(8,128)S(1)} %get-tuple-element.42.state_ref) | copy-start | bytes 22020100
  42.7 17.1 %copy-start.12 = (f32[8,4096]{1,0:T(8,128)}, f32[8,4096]{1,0:T(8,128)S(1)}, u32[]{:S(2)}) copy-start(f32[8,4096]{1,0:T(8,128)S(1)} %get-tuple-element.43.xs_ref) | copy-start | bytes 393220
  42.7 18.6 %copy-start.23 = (bf16[8,4096]{1,0:T(8,128)(2,1)}, bf16[8,4096]{1,0:T(8,128)(2,1)S(1)}, u32[]{:S(2)}) copy-start(bf16[8,4096]{1,0:T(8,128)(2,1)S(1)} %get-tuple-element.45.fresh_ref) | copy-start | bytes 196612
  42.7 6.4 %collective-permute-start.6 = (bf16[8,4096]{1,0:T(8,128)(2,1)S(1)}, bf16[8,4096]{1,0:T(8,128)(2,1)S(1)}, u32[]{:S(2)}, u32[]{:S(2)}) collective-permute-start(bf16[8,4096]{1,0:T(8,128)(2,1)S(1)} %get-tuple-element.37.refs_0_), channel_id=1, source_target_pairs={{0,12},{1,13},{2,14},{3,15},{4,8},{5,9},{6,10},{7,11},{8,4},{9,5},... | collective-permute-start | bytes 196616 | tf_op jit(solution)/shard_map/ppermute | solution.py:42
  46.5 6.0 %collective-permute-start.7 = (bf16[8,4096]{1,0:T(8,128)(2,1)S(1)}, bf16[8,4096]{1,0:T(8,128)(2,1)S(1)}, u32[]{:S(2)}, u32[]{:S(2)}) collective-permute-start(bf16[8,4096]{1,0:T(8,128)(2,1)S(1)} %get-tuple-element.37.refs_0_), channel_id=1, source_target_pairs={{0,8},{1,9},{2,10},{3,11},{4,12},{5,13},{6,14},{7,15},{8,0},{9,1},... | collective-permute-start | bytes 196616 | tf_op jit(solution)/shard_map/ppermute | solution.py:42
  46.5 6.0 %collective-permute-start.8 = (bf16[8,4096]{1,0:T(8,128)(2,1)S(1)}, bf16[8,4096]{1,0:T(8,128)(2,1)S(1)}, u32[]{:S(2)}, u32[]{:S(2)}) collective-permute-start(bf16[8,4096]{1,0:T(8,128)(2,1)S(1)} %get-tuple-element.37.refs_0_), channel_id=1, source_target_pairs={{0,4},{1,5},{2,6},{3,7},{4,0},{5,1},{6,2},{7,3},{8,12},{9,13},{10,... | collective-permute-start | bytes 196616 | tf_op jit(solution)/shard_map/ppermute | solution.py:42
  47.2 5.3 %collective-permute-start.9 = (bf16[8,4096]{1,0:T(8,128)(2,1)S(1)}, bf16[8,4096]{1,0:T(8,128)(2,1)S(1)}, u32[]{:S(2)}, u32[]{:S(2)}) collective-permute-start(bf16[8,4096]{1,0:T(8,128)(2,1)S(1)} %get-tuple-element.37.refs_0_), channel_id=1, source_target_pairs={{0,2},{1,3},{2,0},{3,1},{4,6},{5,7},{6,4},{7,5},{8,10},{9,11},{10,... | collective-permute-start | bytes 196616 | tf_op jit(solution)/shard_map/ppermute | solution.py:42
  49.1 4.3 %collective-permute-start.10 = (bf16[8,4096]{1,0:T(8,128)(2,1)S(1)}, bf16[8,4096]{1,0:T(8,128)(2,1)S(1)}, u32[]{:S(2)}, u32[]{:S(2)}) collective-permute-start(bf16[8,4096]{1,0:T(8,128)(2,1)S(1)} %collective-permute-done.6.refs_1_), channel_id=1, source_target_pairs={{0,2},{1,3},{2,0},{3,1},{4,6},{5,7},{6,4},{7,5},{8,10},{9,11},{10,... | collective-permute-start | bytes 196616 | tf_op jit(solution)/shard_map/ppermute | solution.py:42
  53.4 7.9 %collective-permute-start.12 = (bf16[6,8,4096]{2,1,0:T(8,128)(2,1)S(1)}, bf16[6,8,4096]{2,1,0:T(8,128)(2,1)S(1)}, u32[]{:S(2)}, u32[]{:S(2)}) collective-permute-start(bf16[6,8,4096]{2,1,0:T(8,128)(2,1)S(1)} %join.4.refs_0_), channel_id=1, source_target_pairs={{0,1},{1,0},{2,3},{3,2},{4,5},{5,4},{6,7},{7,6},{8,9},{9,8},{10,11... | collective-permute-start | bytes 1179656 | tf_op jit(solution)/shard_map/ppermute | solution.py:42
  53.5 6.2 %collective-permute-start.11 = (bf16[2,8,4096]{2,1,0:T(8,128)(2,1)S(1)}, bf16[2,8,4096]{2,1,0:T(8,128)(2,1)S(1)}, u32[]{:S(2)}, u32[]{:S(2)}) collective-permute-start(bf16[2,8,4096]{2,1,0:T(8,128)(2,1)S(1)} %join.5), channel_id=1, source_target_pairs={{0,2},{1,3},{2,0},{3,1},{4,6},{5,7},{6,4},{7,5},{8,10},{9,11},{10,... | collective-permute-start | bytes 393224 | tf_op jit(solution)/shard_map/ppermute | solution.py:42
  59.8 1.6 %collective-permute-start.13 = (bf16[2,8,4096]{2,1,0:T(8,128)(2,1)S(1)}, bf16[2,8,4096]{2,1,0:T(8,128)(2,1)S(1)}, u32[]{:S(2)}, u32[]{:S(2)}) collective-permute-start(bf16[2,8,4096]{2,1,0:T(8,128)(2,1)S(1)} %collective-permute-done.11.refs_1_), channel_id=1, source_target_pairs={{0,1},{1,0},{2,3},{3,2},{4,5},{5,4},{6,7},{7,6},{8,9},{9,8},{10,11... | collective-permute-start | bytes 393224 | tf_op jit(solution)/shard_map/ppermute | solution.py:42
  62.0 25.4 %copy-start.8 = (bf16[7,3,4608]{2,0,1:T(8,128)(2,1)S(1)}, bf16[7,3,4608]{2,0,1:T(8,128)(2,1)}, u32[]{:S(2)}) copy-start(bf16[7,3,4608]{2,0,1:T(8,128)(2,1)} %param.25) | copy-start | bytes 580612
  62.0 25.4 %copy-start.13 = (f32[8,4096]{1,0:T(8,128)S(1)}, f32[8,4096]{1,0:T(8,128)}, u32[]{:S(2)}) copy-start(f32[8,4096]{1,0:T(8,128)} %copy-done.12) | copy-start | bytes 393220
  62.0 25.4 %copy-start.24 = (bf16[8,4096]{1,0:T(8,128)(2,1)S(1)}, bf16[8,4096]{1,0:T(8,128)(2,1)}, u32[]{:S(2)}) copy-start(bf16[8,4096]{1,0:T(8,128)(2,1)} %copy-done.23) | copy-start | bytes 196612
  62.0 25.4 %copy-start.26 = (f32[4,7,128]{2,1,0:T(8,128)S(1)}, f32[4,7,128]{2,1,0:T(8,128)}, u32[]{:S(2)}) copy-start(f32[4,7,128]{2,1,0:T(8,128)} %copy-done.25) | copy-start | bytes 43012
  62.0 25.4 %copy-start.32 = (bf16[7,512]{1,0:T(8,128)(2,1)S(1)}, bf16[7,512]{1,0:T(8,128)(2,1)}, u32[]{:S(2)}) copy-start(bf16[7,512]{1,0:T(8,128)(2,1)} %copy-done.31) | copy-start | bytes 21508
  77.8 1.6 %copy-start.3 = (bf16[1,2048,512]{2,1,0:T(8,128)(2,1)S(1)}, bf16[1,2048,512]{2,1,0:T(8,128)(2,1)}, u32[]{:S(2)}) copy-start(bf16[1,2048,512]{2,1,0:T(8,128)(2,1)} %up_ref.1) | copy-start | bytes 6291460
  79.4 1.6 %copy-start.4 = (bf16[1,512,2048]{2,1,0:T(8,128)(2,1)S(1)}, bf16[1,512,2048]{2,1,0:T(8,128)(2,1)}, u32[]{:S(2)}) copy-start(bf16[1,512,2048]{2,1,0:T(8,128)(2,1)} %down_ref.1) | copy-start | bytes 6291460
  83.9 13.5 %all-to-all-start.2 = ((bf16[16,8,1024]{2,1,0:T(8,128)(2,1)}), bf16[16,8,1024]{2,1,0:T(8,128)(2,1)S(1)}, u32[]{:S(2)}, u32[]{:S(2)}) async-start(bf16[16,8,1024]{2,1,0:T(8,128)(2,1)} %get-tuple-element.39), calls=%async_computation.2 | async-start | bytes 524288 | tf_op jit(solution)/shard_map/all_to_all | solution.py:639
  87.5 3.1 %copy-start.1 = (f32[7,64,4096]{2,1,0:T(8,128)S(1)}, f32[7,64,4096]{2,1,0:T(8,128)}, u32[]{:S(2)}) copy-start(f32[7,64,4096]{2,1,0:T(8,128)} %copy-done) | copy-start | bytes 22020100
  (18 other events, 14.5 us)
where the time goes:
time: 99 us; the launch traced here: 98.2 us
  starting transfers between devices  27.7 us (28%)
  local copies, waits for them, and re-layouts  23.8 us (24%)
  Pallas kernels  17.2 us (17%)
  blocking collectives  15.7 us (16%)
  waiting for transfers between devices  12.9 us (13%)
    unnamed x68, local copies, waits for them, and re-layouts  23.8 us
    ppermute x14, starting transfers between devices, swap(): return lax.ppermute(values, 'ep', [(i, i ^ bits) for i in range(count)])  18 us
    all_to_all x1, blocking collectives, body(): slab = lax.all_to_all(slab, 'ep', split_axis=0, concat_axis=0, tiled=True)  15.7 us
    ppermute x14, waiting for transfers between devices, swap(): return lax.ppermute(values, 'ep', [(i, i ^ bits) for i in range(count)])  11.1 us
    all_to_all x1, starting transfers between devices, body(): zx = lax.all_to_all(zx, 'ep', split_axis=0, concat_axis=0, tiled=True)  6.08 us
    pallas_call x1, Pallas kernels, write_state(): call(write_kernel, (jax.ShapeDtypeStruct(state.shape, F32), jax.ShapeDtyp...  5.01 us
    pallas_call x1, Pallas kernels, read_state(): call(read_kernel, (jax.ShapeDtypeStruct(state_in.shape, F32), jax.ShapeDt...  3.86 us
    all_to_all x1, starting transfers between devices, body(): back = lax.all_to_all(back, 'ep', split_axis=0, concat_axis=0, tiled=True)  3.53 us
  transfers between devices with their start and end apart: 16, of which 6 were waited for; matrix products, arithmetic and copies ran while one was open for 0% of the time, Pallas kernels for 13%

commit v1 on v0

--- a/solution.py
+++ b/solution.py
@@ -123,7 +123,7 @@
     hidden_ref, gain_ref, b_ref, c_ref, dt_ref, conv_ref, taps_ref, bias_ref, dt_bias_ref,
     log_ref, skip_ref, ids_ref, prob_ref, score_ref,
     early_ref, coef_ref, step_ref, b_wide_ref, c_wide_ref, decay_ref, bc_ref, ids_out_ref, share_ref,
-    own_ref,
+    own_ref, spread_ref,
 ):
     rows, _ = hidden_ref.shape
     inner = HEADS * HEAD_DIM
@@ -133,13 +133,6 @@
     values = hidden_ref[...].astype(F32)
     scale = lax.rsqrt(jnp.mean(values * values, axis=-1, keepdims=True) + EPS)
     normed = (values * scale * one_row(gain_ref)).astype(BF16)
-    b_part = jnp.dot(normed, b_ref[...], preferred_element_type=F32).astype(BF16)
-    c_part = jnp.dot(normed, c_ref[...], preferred_element_type=F32).astype(BF16)
-    dt_raw = lax.dot_general(
-        normed, dt_ref[...], (((1,), (1,)), ((), ())), preferred_element_type=F32
-    ).astype(BF16)
-    bc_ref[:, :span] = b_part
-    bc_ref[:, span:] = c_part
     taps = taps_ref[...].astype(F32)
     last = taps.shape[0] - 1
     early = one_row(bias_ref)
@@ -147,29 +140,6 @@
         early = early + conv_ref[k].astype(F32) * taps[k : k + 1]
     early_ref[...] = jnp.zeros_like(early_ref)
     early_ref[:rows] = early[:, :inner]
-    fresh = jnp.concatenate([b_part, c_part], axis=1).astype(F32)
-    active = silu(early[:, inner:] + fresh * taps[last:, inner:])
-    b_act = active[:, :span]
-    c_act = active[:, span:]
-    step = jax.nn.softplus(dt_raw.astype(F32) + dt_bias_ref[...])
-    decay = jnp.exp(-step * jnp.exp(log_ref[...]))
-    coefs = []
-    for g in range(SSM_GROUPS):
-        cut = slice(g * STATE, (g + 1) * STATE)
-        b_wide_ref[g] = jnp.concatenate([b_act[:, cut]] * (LANES // STATE), axis=1)
-        c_wide_ref[g] = jnp.concatenate([c_act[:, cut]] * (LANES // STATE), axis=1)
-        dots = jnp.sum(b_act[:, cut] * c_act[:, cut], axis=1, keepdims=True)
-        coefs.append(jnp.broadcast_to(dots, (rows, per_group)))
-    coef = step * jnp.concatenate(coefs, axis=1) + skip_ref[...]
-    chan = lax.broadcasted_iota(jnp.int32, (3 * HEADS, inner), 0)
-    lane = lax.broadcasted_iota(jnp.int32, (3 * HEADS, inner), 1)
-    spread = (lane // HEAD_DIM == chan % HEADS).astype(F32).astype(BF16)
-    for values, ref in ((coef, coef_ref), (step, step_ref)):
-        parts = jnp.concatenate(three_parts(values), axis=1)
-        ref[...] = jnp.zeros_like(ref)
-        ref[:rows] = jnp.dot(parts, spread, preferred_element_type=F32)
-    for t in range(rows):
-        decay_ref[t] = jnp.broadcast_to(to_column(decay[t : t + 1], HEADS), (HEADS, LANES))
     width = share_ref.shape[1]
     split = share_ref.shape[0] // (3 * PAD)
     at = lax.broadcasted_iota(jnp.int32, (rows, width), 1)
@@ -201,13 +171,47 @@
         cut = jnp.where(at % split == s, weight, 0.0)
         for i, part in enumerate(three_parts(cut)):
             share_ref[(3 * s + i) * PAD : (3 * s + i) * PAD + rows] = part
+    chan = lax.broadcasted_iota(jnp.int32, (HEADS, inner), 0)
+    lane = lax.broadcasted_iota(jnp.int32, (HEADS, inner), 1)
+    spread_ref[...] = (lane // HEAD_DIM == chan).astype(F32).astype(BF16)
+    b_part = jnp.dot(normed, b_ref[...], preferred_element_type=F32).astype(BF16)
+    c_part = jnp.dot(normed, c_ref[...], preferred_element_type=F32).astype(BF16)
+    dt_raw = lax.dot_general(
+        normed, dt_ref[...], (((1,), (1,)), ((), ())), preferred_element_type=F32
+    ).astype(BF16)
+    bc_ref[:, :span] = b_part
+    bc_ref[:, span:] = c_part
+    fresh = jnp.concatenate([b_part, c_part], axis=1).astype(F32)
+    active = silu(early[:, inner:] + fresh * taps[last:, inner:])
+    b_act = active[:, :span]
+    c_act = active[:, span:]
+    step = jax.nn.softplus(dt_raw.astype(F32) + dt_bias_ref[...])
+    decay = jnp.exp(-step * jnp.exp(log_ref[...]))
+    coefs = []
+    for g in range(SSM_GROUPS):
+        cut = slice(g * STATE, (g + 1) * STATE)
+        b_wide_ref[g] = jnp.concatenate([b_act[:, cut]] * (LANES // STATE), axis=1)
+        c_wide_ref[g] = jnp.concatenate([c_act[:, cut]] * (LANES // STATE), axis=1)
+        dots = jnp.sum(b_act[:, cut] * c_act[:, cut], axis=1, keepdims=True)
+        coefs.append(jnp.broadcast_to(dots, (rows, per_group)))
+    coef = step * jnp.concatenate(coefs, axis=1) + skip_ref[...]
+    blank = jnp.zeros((PAD - rows, HEADS), F32)
+    parts = []
+    for values in (coef, step):
+        parts += three_parts(jnp.concatenate([values, blank], axis=0))
+    wide = jnp.dot(jnp.concatenate(parts, axis=0), spread_ref[...], preferred_element_type=F32)
+    for i, ref in enumerate((coef_ref, step_ref)):
+        at = 3 * PAD * i
+        ref[...] = wide[at : at + PAD] + wide[at + PAD : at + 2 * PAD] + wide[at + 2 * PAD : at + 3 * PAD]
+    for t in range(rows):
+        decay_ref[t] = jnp.broadcast_to(to_column(decay[t : t + 1], HEADS), (HEADS, LANES))
 
 
 def read_kernel(
-    state_ref, c_ref, decay_ref, keep_ref, out_ref, c_wide_ref, sums_ref, flat_ref, sems
+    state_ref, c_ref, decay_ref, out_ref, keep_ref, c_wide_ref, sums_ref, flat_ref, sems
 ):
     rows, heads, width = state_ref.shape
-    lanes = 512
+    lanes = 1024
 
     def copy(chunk):
         cut = pl.ds(pl.multiple_of(chunk * lanes, lanes), lanes)
@@ -249,20 +253,18 @@
     rows, heads, width = state_in.shape
     return call(
         read_kernel,
-        (
-            jax.ShapeDtypeStruct(state_in.shape, F32),
-            jax.ShapeDtypeStruct((PAD, heads * HEAD_DIM), F32),
-        ),
-        12,
+        jax.ShapeDtypeStruct((PAD, heads * HEAD_DIM), F32),
+        20,
         20_000_000,
         state_in.size * 4,
         in_specs=[pl.BlockSpec(memory_space=pltpu.HBM), vmem(), vmem()],
-        out_specs=(vmem(), vmem()),
+        out_specs=vmem(),
         scratch_shapes=[
+            pltpu.VMEM(state_in.shape, F32),
             pltpu.VMEM((rows, heads, LANES), F32),
             pltpu.VMEM((rows * heads, HEAD_DIM), F32),
             pltpu.VMEM((rows * heads, HEAD_DIM), F32),
-            pltpu.SemaphoreType.DMA((width // 512,)),
+            pltpu.SemaphoreType.DMA((width // 1024,)),
         ],
         name="read_state",
     )(state_in, c_wide, decay_wide)
@@ -270,11 +272,23 @@
 
 def write_kernel(
     state_ref, xs_ref, b_ref, decay_ref, conv_ref, fresh_ref, bc_ref,
-    out_ref, conv_out_ref, parts_ref, b_wide_ref, new_ref, sems,
+    out_ref, conv_out_ref, parts_ref, b_wide_ref, new_ref, in_sems, sems,
 ):
     rows, heads, width = state_ref.shape
     lanes = 512
     inner = heads * HEAD_DIM
+
+    def fetch(chunk):
+        cut = pl.ds(pl.multiple_of(chunk * lanes, lanes), lanes)
+        return pltpu.make_async_copy(
+            state_ref.at[:, :, cut], new_ref.at[:, :, cut], in_sems.at[chunk]
+        )
+
+    def begin(chunk, carry):
+        fetch(chunk).start()
+        return carry
+
+    lax.fori_loop(0, width // lanes, begin, 0)
     for h in range(heads):
         parts_ref[pl.ds(h, rows, stride=heads), :] = xs_ref[
             :rows, h * HEAD_DIM : (h + 1) * HEAD_DIM
@@ -295,10 +309,11 @@
         spread = chunk * (lanes // STATE) + lane // STATE == chan % HEAD_DIM
         wide = jnp.dot(parts, spread.astype(F32).astype(BF16), preferred_element_type=F32)
         wide = wide.reshape(rows, heads, lanes)
+        fetch(chunk).wait()
         for k in range(lanes // LANES):
             cut = pl.ds(at + k * LANES, LANES)
             new_ref[:, :, cut] = (
-                decay_ref[...] * state_ref[:, :, cut]
+                decay_ref[...] * new_ref[:, :, cut]
                 + wide[:, :, k * LANES : (k + 1) * LANES] * b_wide_ref[...]
             )
         copy(chunk).start()
@@ -325,13 +340,14 @@
         (jax.ShapeDtypeStruct(state.shape, F32), jax.ShapeDtypeStruct(conv.shape, BF16)),
         16,
         40_000_000,
-        state.size * 4,
-        in_specs=[vmem()] * 7,
+        state.size * 8,
+        in_specs=[pl.BlockSpec(memory_space=pltpu.HBM)] + [vmem()] * 6,
         out_specs=(pl.BlockSpec(memory_space=pltpu.HBM), vmem()),
         scratch_shapes=[
             pltpu.VMEM((rows * heads, HEAD_DIM), F32),
             pltpu.VMEM((rows, heads, LANES), F32),
             pltpu.VMEM(state.shape, F32),
+            pltpu.SemaphoreType.DMA((width // 512,)),
             pltpu.SemaphoreType.DMA((width // 512,)),
         ],
         name="write_state",
@@ -538,6 +554,7 @@
         4_000_000,
         in_specs=[vmem()] * 14,
         out_specs=(vmem(),) * 10,
+        scratch_shapes=[pltpu.VMEM((HEADS, inner), BF16)],
         name="local",
     )(
         *[
@@ -561,7 +578,7 @@
         ]
     )
     parts = gather(hidden, count, AHEAD["first"], own)
-    state, read = read_state(streamed(state_in), c_wide, decay_wide)
+    read = read_state(streamed(state_in), c_wide, decay_wide)
 
     cols = z_weight.shape[1]
     zx, all_rows = call(
@@ -606,7 +623,7 @@
 
     parts = gather(y_mix, count, AHEAD["second"])
     state_out, conv_out = write_state(
-        state, xs, b_wide, decay_wide, conv_state, x_fresh, bc
+        streamed(state_in), xs, b_wide, decay_wide, conv_state, x_fresh, bc
     )
     out_cols = out_weight.shape[1]
     slab = call(

time: 99 us -> 85.3 us (0.86)
  local copies, waits for them, and re-layouts: 23.8 us -> 6.88 us
  waiting for transfers between devices: 12.9 us -> 23.6 us
  starting transfers between devices: 27.7 us -> 20.3 us
  Pallas kernels: 17.2 us -> 20.4 us
  blocking collectives: 15.7 us -> 12.7 us
    unnamed x68 -> x58, local copies, waits for them, and re-layouts: 23.8 us -> 6.88 us
    ppermute x14, waiting for transfers between devices: 11.1 us -> 18.2 us  [swap(): return lax.ppermute(values, 'ep', [(i, i ^ bits) for i in range(count)])]
    ppermute x14, starting transfers between devices: 18 us -> 12.3 us  [swap(): return lax.ppermute(values, 'ep', [(i, i ^ bits) for i in range(count)])]
    all_to_all x1, waiting for transfers between devices: 0.01 us -> 3.28 us  [body(): zx = lax.all_to_all(zx, 'ep', split_axis=0, concat_axis=0, tiled=True)]
    all_to_all x1, blocking collectives: 15.7 us -> 12.7 us  [body(): slab = lax.all_to_all(slab, 'ep', split_axis=0, concat_axis=0, tiled=True)]
    pallas_call x1, Pallas kernels: 5.01 us -> 7.82 us  [write_state(): call(write_kernel, (jax.ShapeDtypeStruct(state.shape, F32), jax.ShapeDtyp...]
    all_to_all x1, starting transfers between devices: 6.08 us -> 4.45 us  [body(): zx = lax.all_to_all(zx, 'ep', split_axis=0, concat_axis=0, tiled=True)]
  transfers between devices with their start and end apart: 16 -> 16, of which waited for: 6 -> 10; matrix products, arithmetic and copies ran while one was open for 0% -> 0% of each run, Pallas kernels for 13% -> 18%
where the time goes in v1:
time: 85.3 us; the launch traced here: 84.7 us
  waiting for transfers between devices  23.6 us (28%)
  Pallas kernels  20.4 us (24%)
  starting transfers between devices  20.3 us (24%)
  blocking collectives  12.7 us (15%)
  local copies, waits for them, and re-layouts  6.88 us (8%)
  between operations  1.01 us (1%)
    ppermute x14, waiting for transfers between devices, swap(): return lax.ppermute(values, 'ep', [(i, i ^ bits) for i in range(count)])  18.2 us
    all_to_all x1, blocking collectives, body(): slab = lax.all_to_all(slab, 'ep', split_axis=0, concat_axis=0, tiled=True)  12.7 us
    ppermute x14, starting transfers between devices, swap(): return lax.ppermute(values, 'ep', [(i, i ^ bits) for i in range(count)])  12.3 us
    pallas_call x1, Pallas kernels, write_state(): call(write_kernel, (jax.ShapeDtypeStruct(state.shape, F32), jax.ShapeDtyp...  7.82 us
    unnamed x58, local copies, waits for them, and re-layouts  6.88 us
    all_to_all x1, starting transfers between devices, body(): zx = lax.all_to_all(zx, 'ep', split_axis=0, concat_axis=0, tiled=True)  4.45 us
    pallas_call x1, Pallas kernels, read_state(): call(read_kernel, jax.ShapeDtypeStruct((PAD, heads * HEAD_DIM), F32), 20,...  3.94 us
    all_to_all x1, starting transfers between devices, body(): back = lax.all_to_all(back, 'ep', split_axis=0, concat_axis=0, tiled=True)  3.53 us
  transfers between devices with their start and end apart: 16, of which 10 were waited for; matrix products, arithmetic and copies ran while one was open for 0% of the time, Pallas kernels for 18%

profile of v1, /device:TPU:0, one launch (start us, length us, event | category | flops | bytes accessed | tf_op | source)
XLA Modules:
  0.0 84.7 jit_solution(7602528601151542565)
XLA Ops:
  0.7 5.1 %collective-permute-start = (bf16[7,2048]{1,0:T(8,128)(2,1)}, bf16[7,2048]{1,0:T(8,128)(2,1)S(1)}, u32[]{:S(2)}, u32[]{:S(2)}) collective-permute-start(bf16[7,2048]{1,0:T(8,128)(2,1)} %hidden_ref.1), channel_id=1, source_target_pairs={{0,12},{1,13},{2,14},{3,15},{4,8},{5,9},{6,10},{7,11},{8,4},{9,5},... | collective-permute-start | bytes 86024 | tf_op jit(solution)/shard_map/ppermute | solution.py:42
  5.8 0.6 collective-permute-start.1
  6.5 2.8 %local.1 = (f32[8,4096]{1,0:T(8,128)S(1)}, f32[8,4096]{1,0:T(8,128)S(1)}, f32[8,4096]{1,0:T(8,128)S(1)}, f32[4,7,128]{2,1,0:T(8,128)S(1)}, f32[4,7,128]{2,1,0:T(...) custom-call(bf16[7,2048]{1,0:T(8,128)(2,1)} %hidden_ref.1, ...), custom_call_target="tpu_custom_call" | custom-call | flops 10000000 | bytes 4000000 | tf_op jit(solution)/shard_map/local/pallas_call | solution.py:538
  9.9 1.0 %collective-permute-done.1.refs_2_ = bf16[7,2048]{1,0:T(8,128)(2,1)S(1)} collective-permute-done((bf16[7,2048]{1,0:T(8,128)(2,1)}, bf16[7,2048]{1,0:T(8,128)(2,1)S(1)}, u32[]{:S(2)}, u32[]{:S(2)}) %collective-permute-start.1) | collective-permute-done | bytes 28704 | tf_op jit(solution)/shard_map/ppermute | solution.py:42
  11.0 1.6 %collective-permute-start.3 = (bf16[4,7,2048]{2,1,0:T(8,128)(2,1)S(1)}, bf16[4,7,2048]{2,1,0:T(8,128)(2,1)S(1)}, u32[]{:S(2)}, u32[]{:S(2)}) collective-permute-start(bf16[4,7,2048]{2,1,0:T(8,128)(2,1)S(1)} %join.3.refs_0_), channel_id=1, source_target_pairs={{0,2},{1,3},{2,0},{3,1},{4,6},{5,7},{6,4},{7,5},{8,10},{9,11},{10,... | collective-permute-start | bytes 344072 | tf_op jit(solution)/shard_map/ppermute | solution.py:42
  12.6 3.4 %collective-permute-done.3.refs_1_ = bf16[4,7,2048]{2,1,0:T(8,128)(2,1)S(1)} collective-permute-done((bf16[4,7,2048]{2,1,0:T(8,128)(2,1)S(1)}, bf16[4,7,2048]{2,1,0:T(8,128)(2,1)S(1)}, u32[]{:S(2)}, u32[]{:S(2)}) %collective-permute-start.3) | collective-permute-done | bytes 114720 | tf_op jit(solution)/shard_map/ppermute | solution.py:42
  16.0 1.3 %collective-permute-done.5.refs_3_ = bf16[4,7,2048]{2,1,0:T(8,128)(2,1)S(1)} collective-permute-done((bf16[4,7,2048]{2,1,0:T(8,128)(2,1)S(1)}, bf16[4,7,2048]{2,1,0:T(8,128)(2,1)S(1)}, u32[]{:S(2)}, u32[]{:S(2)}) %collective-permute-start.5) | collective-permute-done | bytes 114720 | tf_op jit(solution)/shard_map/ppermute | solution.py:42
  17.4 1.4 %project.1 = (bf16[16,8,512]{2,1,0:T(8,128)(2,1)}, bf16[16,8,2048]{2,1,0:T(8,128)(2,1)S(1)}) custom-call(bf16[4,7,2048]{2,1,0:T(8,128)(2,1)S(1)} %join.3.refs_0_, bf16[4,7,2048]{2,1,0:T(8,128)(2,1)S(1)} %collective-permute-done.3.refs_1_, bf16[4,7,2048]{2,1,0:T(8,128)(2,1)S(1)} %collective-permute-done.4.refs_2_, ...), custom_call_target="tpu_custom_call" | custom-call | flops 268435456 | bytes 2097152 | tf_op jit(solution)/shard_map/project/pallas_call | solution.py:584
  18.8 0.8 copy-done.9
  19.6 4.5 %all-to-all-start = ((bf16[16,8,512]{2,1,0:T(8,128)(2,1)}), bf16[16,8,512]{2,1,0:T(8,128)(2,1)S(1)}, u32[]{:S(2)}, u32[]{:S(2)}) async-start(bf16[16,8,512]{2,1,0:T(8,128)(2,1)} %get-tuple-element.26), calls=%async_computation | async-start | bytes 262144 | tf_op jit(solution)/shard_map/all_to_all | solution.py:597
  24.1 3.9 %read_state.1.read_ref = f32[8,4096]{1,0:T(8,128)S(1)} custom-call(f32[7,64,4096]{2,1,0:T(8,128)} %state_ref.3, f32[4,7,128]{2,1,0:T(8,128)S(1)} %get-tuple-element.31.c_ref, f32[7,64,128]{2,1,0:T(8,128)S(1)} %get-tuple-element.32.decay_ref), custom_call_target="tpu_custom_call" | custom-call | flops 20000000 | bytes 7340032 | tf_op jit(solution)/shard_map/read_state/pallas_call | solution.py:254
  28.0 0.6 copy-done.7
  28.7 3.3 %all-to-all-done.zx_ref = bf16[16,8,512]{2,1,0:T(8,128)(2,1)S(1)} async-done(((bf16[16,8,512]{2,1,0:T(8,128)(2,1)}), bf16[16,8,512]{2,1,0:T(8,128)(2,1)S(1)}, u32[]{:S(2)}, u32[]{:S(2)}) %all-to-all-start) | async-done | bytes 131104 | tf_op jit(solution)/shard_map/all_to_all | solution.py:597
  31.9 0.9 %copy-done.8 = f32[8,4096]{1,0:T(8,128)S(1)} copy-done((f32[8,4096]{1,0:T(8,128)S(1)}, f32[8,4096]{1,0:T(8,128)}, u32[]{:S(2)}) %copy-start.8) | copy-done | bytes 131096
  32.8 0.9 %copy-done.15 = f32[8,4096]{1,0:T(8,128)S(1)} copy-done((f32[8,4096]{1,0:T(8,128)S(1)}, f32[8,4096]{1,0:T(8,128)}, u32[]{:S(2)}) %copy-start.15) | copy-done | bytes 131096
  33.8 0.9 %copy-done.17 = f32[8,4096]{1,0:T(8,128)S(1)} copy-done((f32[8,4096]{1,0:T(8,128)S(1)}, f32[8,4096]{1,0:T(8,128)}, u32[]{:S(2)}) %copy-start.17) | copy-done | bytes 131096
  34.7 0.9 %copy-done.19 = f32[8,4096]{1,0:T(8,128)S(1)} copy-done((f32[8,4096]{1,0:T(8,128)S(1)}, f32[8,4096]{1,0:T(8,128)}, u32[]{:S(2)}) %copy-start.19) | copy-done | bytes 131096
  35.6 0.7 copy-done.25
  36.5 0.8 collective-permute-start.6
  37.3 1.2 %collective-permute-start.9 = (bf16[8,4096]{1,0:T(8,128)(2,1)S(1)}, bf16[8,4096]{1,0:T(8,128)(2,1)S(1)}, u32[]{:S(2)}, u32[]{:S(2)}) collective-permute-start(bf16[8,4096]{1,0:T(8,128)(2,1)S(1)} %get-tuple-element.34.refs_0_), channel_id=1, source_target_pairs={{0,2},{1,3},{2,0},{3,1},{4,6},{5,7},{6,4},{7,5},{8,10},{9,11},{10,... | collective-permute-start | bytes 196616 | tf_op jit(solution)/shard_map/ppermute | solution.py:42
  38.6 2.4 %collective-permute-start.7 = (bf16[8,4096]{1,0:T(8,128)(2,1)S(1)}, bf16[8,4096]{1,0:T(8,128)(2,1)S(1)}, u32[]{:S(2)}, u32[]{:S(2)}) collective-permute-start(bf16[8,4096]{1,0:T(8,128)(2,1)S(1)} %get-tuple-element.34.refs_0_), channel_id=1, source_target_pairs={{0,8},{1,9},{2,10},{3,11},{4,12},{5,13},{6,14},{7,15},{8,0},{9,1},... | collective-permute-start | bytes 196616 | tf_op jit(solution)/shard_map/ppermute | solution.py:42
  41.0 1.9 %collective-permute-done.6.refs_1_ = bf16[8,4096]{1,0:T(8,128)(2,1)S(1)} collective-permute-done((bf16[8,4096]{1,0:T(8,128)(2,1)S(1)}, bf16[8,4096]{1,0:T(8,128)(2,1)S(1)}, u32[]{:S(2)}, u32[]{:S(2)}) %collective-permute-start.6) | collective-permute-done | bytes 65568 | tf_op jit(solution)/shard_map/ppermute | solution.py:42
  43.0 1.5 %collective-permute-done.8.refs_3_.refs_1_ = bf16[8,4096]{1,0:T(8,128)(2,1)S(1)} collective-permute-done((bf16[8,4096]{1,0:T(8,128)(2,1)S(1)}, bf16[8,4096]{1,0:T(8,128)(2,1)S(1)}, u32[]{:S(2)}, u32[]{:S(2)}) %collective-permute-start.8) | collective-permute-done | bytes 65568 | tf_op jit(solution)/shard_map/ppermute | solution.py:42
  44.5 2.6 %collective-permute-done.10.refs_5_ = bf16[8,4096]{1,0:T(8,128)(2,1)S(1)} collective-permute-done((bf16[8,4096]{1,0:T(8,128)(2,1)S(1)}, bf16[8,4096]{1,0:T(8,128)(2,1)S(1)}, u32[]{:S(2)}, u32[]{:S(2)}) %collective-permute-start.10) | collective-permute-done | bytes 65568 | tf_op jit(solution)/shard_map/ppermute | solution.py:42
  47.5 5.7 %collective-permute-done.11.refs_1_ = bf16[2,8,4096]{2,1,0:T(8,128)(2,1)S(1)} collective-permute-done((bf16[2,8,4096]{2,1,0:T(8,128)(2,1)S(1)}, bf16[2,8,4096]{2,1,0:T(8,128)(2,1)S(1)}, u32[]{:S(2)}, u32[]{:S(2)}) %collective-permute-start.11) | collective-permute-done | bytes 131104 | tf_op jit(solution)/shard_map/ppermute | solution.py:42
  53.2 1.0 %copy-done.10 = bf16[16,8,2048]{2,1,0:T(8,128)(2,1)S(1)} copy-done((bf16[16,8,2048]{2,1,0:T(8,128)(2,1)S(1)}, bf16[16,8,2048]{2,1,0:T(8,128)(2,1)}, u32[]{:S(2)}) %copy-start.10) | copy-done | bytes 524312
  55.5 12.7 %all_to_all.15.cols_ref = bf16[16,56,128]{2,1,0:T(8,128)(2,1)S(1)} all-to-all(bf16[16,56,128]{2,1,0:T(8,128)(2,1)S(1)} %output.1), channel_id=1, replica_groups=mesh['grp'=2,'ep'=16] {'ep'}, dimensions={0} | all-to-all | bytes 458752 | tf_op jit(solution)/shard_map/all_to_all | solution.py:641
  68.2 2.2 %expert.1 = (bf16[16,8,1024]{2,1,0:T(8,128)(2,1)}, bf16[8,2048]{1,0:T(8,128)(2,1)S(1)}) custom-call(bf16[56,2048]{1,0:T(8,128)(2,1)S(1)} %get-tuple-element.28.hidden_ref, bf16[16,56,128]{2,1,0:T(8,128)(2,1)S(1)} %all_to_all.15.cols_ref, bf16[16,128]{1,0:T(8,128)(2,1)S(1)} %bitcast.18, bf16[1,2048,512]{2,1,0:T(8,128)(2,1)S(1)} %copy-done, ...), custom_call_target="tpu_custom_call" | custom-call | flops 805306368 | bytes 6291456 | tf_op jit(solution)/shard_map/expert/pallas_call | solution.py:642
  70.4 3.5 %all-to-all-start.2 = ((bf16[16,8,1024]{2,1,0:T(8,128)(2,1)}), bf16[16,8,1024]{2,1,0:T(8,128)(2,1)S(1)}, u32[]{:S(2)}, u32[]{:S(2)}) async-start(bf16[16,8,1024]{2,1,0:T(8,128)(2,1)} %get-tuple-element.36), calls=%async_computation.2 | async-start | bytes 524288 | tf_op jit(solution)/shard_map/all_to_all | solution.py:656
  74.0 7.8 %write_state.1 = (f32[7,64,4096]{2,1,0:T(8,128)}, bf16[3,7,4608]{2,1,0:T(8,128)(2,1)}) custom-call(f32[7,64,4096]{2,1,0:T(8,128)} %state_ref.3, f32[8,4096]{1,0:T(8,128)S(1)} %copy-done.13, f32[4,7,128]{2,1,0:T(8,128)S(1)} %copy-done.23, f32[7,64,128]{2,1,0:T(8,128)S(1)} %get-tuple-element.32.decay_ref, bf16[3,7,4608]{2,1,0:T(8,128)(2,1)S(1)} %bitcast.14, ...), custom_call_target="tpu_custom_call" | custom-call | flops 40000000 | bytes 14680064 | tf_op jit(solution)/shard_map/write_state/pallas_call | solution.py:338
  81.8 2.1 %all-to-all-done.2.back_ref = bf16[16,8,1024]{2,1,0:T(8,128)(2,1)S(1)} async-done(((bf16[16,8,1024]{2,1,0:T(8,128)(2,1)}), bf16[16,8,1024]{2,1,0:T(8,128)(2,1)S(1)}, u32[]{:S(2)}, u32[]{:S(2)}) %all-to-all-start.2) | async-done | bytes 262176 | tf_op jit(solution)/shard_map/all_to_all | solution.py:656
  83.9 0.8 combine.1
  (71 shorter events, 2.6 us)
Async XLA Ops:
  0.6 16.7 %copy-start.24 = (bf16[2048]{0:T(1024)(128)(2,1)S(1)}, bf16[2048]{0:T(1024)(128)(2,1)}, u32[]{:S(2)}) copy-start(bf16[2048]{0:T(1024)(128)(2,1)} %param.29) | copy-start | bytes 12292
  0.6 16.7 %copy-start.4 = (bf16[2048,256]{1,0:T(8,128)(2,1)S(1)}, bf16[2048,256]{1,0:T(8,128)(2,1)}, u32[]{:S(2)}) copy-start(bf16[2048,256]{1,0:T(8,128)(2,1)} %refs_5_.1) | copy-start | bytes 3145732
  0.7 16.7 %copy-start.3 = (bf16[2048,256]{1,0:T(8,128)(2,1)S(1)}, bf16[2048,256]{1,0:T(8,128)(2,1)}, u32[]{:S(2)}) copy-start(bf16[2048,256]{1,0:T(8,128)(2,1)} %refs_4_.2) | copy-start | bytes 3145732
  0.7 8.6 %collective-permute-start = (bf16[7,2048]{1,0:T(8,128)(2,1)}, bf16[7,2048]{1,0:T(8,128)(2,1)S(1)}, u32[]{:S(2)}, u32[]{:S(2)}) collective-permute-start(bf16[7,2048]{1,0:T(8,128)(2,1)} %hidden_ref.1), channel_id=1, source_target_pairs={{0,12},{1,13},{2,14},{3,15},{4,8},{5,9},{6,10},{7,11},{8,4},{9,5},... | collective-permute-start | bytes 86024 | tf_op jit(solution)/shard_map/ppermute | solution.py:42
  5.8 4.1 %collective-permute-start.2 = (bf16[7,2048]{1,0:T(8,128)(2,1)}, bf16[7,2048]{1,0:T(8,128)(2,1)S(1)}, u32[]{:S(2)}, u32[]{:S(2)}) collective-permute-start(bf16[7,2048]{1,0:T(8,128)(2,1)} %hidden_ref.1), channel_id=1, source_target_pairs={{0,4},{1,5},{2,6},{3,7},{4,0},{5,1},{6,2},{7,3},{8,12},{9,13},{10,... | collective-permute-start | bytes 86024 | tf_op jit(solution)/shard_map/ppermute | solution.py:42
  5.8 5.1 %collective-permute-start.1 = (bf16[7,2048]{1,0:T(8,128)(2,1)}, bf16[7,2048]{1,0:T(8,128)(2,1)S(1)}, u32[]{:S(2)}, u32[]{:S(2)}) collective-permute-start(bf16[7,2048]{1,0:T(8,128)(2,1)} %hidden_ref.1), channel_id=1, source_target_pairs={{0,8},{1,9},{2,10},{3,11},{4,12},{5,13},{6,14},{7,15},{8,0},{9,1},... | collective-permute-start | bytes 86024 | tf_op jit(solution)/shard_map/ppermute | solution.py:42
  9.2 9.5 %copy-start.14 = (f32[8,4096]{1,0:T(8,128)}, f32[8,4096]{1,0:T(8,128)S(1)}, u32[]{:S(2)}) copy-start(f32[8,4096]{1,0:T(8,128)S(1)} %get-tuple-element.29.early_ref) | copy-start | bytes 393220
  9.2 9.5 %copy-start.16 = (f32[8,4096]{1,0:T(8,128)}, f32[8,4096]{1,0:T(8,128)S(1)}, u32[]{:S(2)}) copy-start(f32[8,4096]{1,0:T(8,128)S(1)} %get-tuple-element.30.coef_ref) | copy-start | bytes 393220
  9.3 9.5 %copy-start.18 = (f32[8,4096]{1,0:T(8,128)}, f32[8,4096]{1,0:T(8,128)S(1)}, u32[]{:S(2)}) copy-start(f32[8,4096]{1,0:T(8,128)S(1)} %get-tuple-element.33.step_ref) | copy-start | bytes 393220
  9.3 9.5 %copy-start.22 = (f32[4,7,128]{2,1,0:T(8,128)}, f32[4,7,128]{2,1,0:T(8,128)S(1)}, u32[]{:S(2)}) copy-start(f32[4,7,128]{2,1,0:T(8,128)S(1)} %get-tuple-element.40.b_ref) | copy-start | bytes 43012
  9.3 9.5 %copy-start.26 = (bf16[7,512]{1,0:T(8,128)(2,1)}, bf16[7,512]{1,0:T(8,128)(2,1)S(1)}, u32[]{:S(2)}) copy-start(bf16[7,512]{1,0:T(8,128)(2,1)S(1)} %get-tuple-element.42.bc_ref) | copy-start | bytes 21508
  11.0 5.0 %collective-permute-start.3 = (bf16[4,7,2048]{2,1,0:T(8,128)(2,1)S(1)}, bf16[4,7,2048]{2,1,0:T(8,128)(2,1)S(1)}, u32[]{:S(2)}, u32[]{:S(2)}) collective-permute-start(bf16[4,7,2048]{2,1,0:T(8,128)(2,1)S(1)} %join.3.refs_0_), channel_id=1, source_target_pairs={{0,2},{1,3},{2,0},{3,1},{4,6},{5,7},{6,4},{7,5},{8,10},{9,11},{10,... | collective-permute-start | bytes 344072 | tf_op jit(solution)/shard_map/ppermute | solution.py:42
  12.6 3.5 %collective-permute-start.4 = (bf16[4,7,2048]{2,1,0:T(8,128)(2,1)S(1)}, bf16[4,7,2048]{2,1,0:T(8,128)(2,1)S(1)}, u32[]{:S(2)}, u32[]{:S(2)}) collective-permute-start(bf16[4,7,2048]{2,1,0:T(8,128)(2,1)S(1)} %join.3.refs_0_), channel_id=1, source_target_pairs={{0,1},{1,0},{2,3},{3,2},{4,5},{5,4},{6,7},{7,6},{8,9},{9,8},{10,11... | collective-permute-start | bytes 344072 | tf_op jit(solution)/shard_map/ppermute | solution.py:42
  16.0 1.3 %collective-permute-start.5 = (bf16[4,7,2048]{2,1,0:T(8,128)(2,1)S(1)}, bf16[4,7,2048]{2,1,0:T(8,128)(2,1)S(1)}, u32[]{:S(2)}, u32[]{:S(2)}) collective-permute-start(bf16[4,7,2048]{2,1,0:T(8,128)(2,1)S(1)} %collective-permute-done.3.refs_1_), channel_id=1, source_target_pairs={{0,1},{1,0},{2,3},{3,2},{4,5},{5,4},{6,7},{7,6},{8,9},{9,8},{10,11... | collective-permute-start | bytes 344072 | tf_op jit(solution)/shard_map/ppermute | solution.py:42
  19.6 12.4 %all-to-all-start = ((bf16[16,8,512]{2,1,0:T(8,128)(2,1)}), bf16[16,8,512]{2,1,0:T(8,128)(2,1)S(1)}, u32[]{:S(2)}, u32[]{:S(2)}) async-start(bf16[16,8,512]{2,1,0:T(8,128)(2,1)} %get-tuple-element.26), calls=%async_computation | async-start | bytes 262144 | tf_op jit(solution)/shard_map/all_to_all | solution.py:597
  24.0 7.9 %copy-start.11 = (bf16[4,4608]{1,0:T(4,128)(2,1)S(1)}, bf16[4,4608]{1,0:T(4,128)(2,1)}, u32[]{:S(2)}) copy-start(bf16[4,4608]{1,0:T(4,128)(2,1)} %taps_ref.3) | copy-start | bytes 110596
  24.0 44.1 %copy-start.2 = (bf16[1,512,2048]{2,1,0:T(8,128)(2,1)S(1)}, bf16[1,512,2048]{2,1,0:T(8,128)(2,1)}, u32[]{:S(2)}) copy-start(bf16[1,512,2048]{2,1,0:T(8,128)(2,1)} %down_ref.1) | copy-start | bytes 6291460
  28.7 26.2 %copy-start.5 = (bf16[4096,128]{1,0:T(8,128)(2,1)S(1)}, bf16[4096,128]{1,0:T(8,128)(2,1)}, u32[]{:S(2)}) copy-start(bf16[4096,128]{1,0:T(8,128)(2,1)} %refs_4_.3) | copy-start | bytes 3145732
  36.5 16.7 %copy-start.20 = (bf16[8,4096]{1,0:T(8,128)(2,1)}, bf16[8,4096]{1,0:T(8,128)(2,1)S(1)}, u32[]{:S(2)}) copy-start(bf16[8,4096]{1,0:T(8,128)(2,1)S(1)} %get-tuple-element.41.fresh_ref) | copy-start | bytes 196612
  36.5 18.3 %copy-start.12 = (f32[8,4096]{1,0:T(8,128)}, f32[8,4096]{1,0:T(8,128)S(1)}, u32[]{:S(2)}) copy-start(f32[8,4096]{1,0:T(8,128)S(1)} %get-tuple-element.39.xs_ref) | copy-start | bytes 393220
  36.5 6.3 %collective-permute-start.6 = (bf16[8,4096]{1,0:T(8,128)(2,1)S(1)}, bf16[8,4096]{1,0:T(8,128)(2,1)S(1)}, u32[]{:S(2)}, u32[]{:S(2)}) collective-permute-start(bf16[8,4096]{1,0:T(8,128)(2,1)S(1)} %get-tuple-element.34.refs_0_), channel_id=1, source_target_pairs={{0,12},{1,13},{2,14},{3,15},{4,8},{5,9},{6,10},{7,11},{8,4},{9,5},... | collective-permute-start | bytes 196616 | tf_op jit(solution)/shard_map/ppermute | solution.py:42
  37.3 5.7 %collective-permute-start.9 = (bf16[8,4096]{1,0:T(8,128)(2,1)S(1)}, bf16[8,4096]{1,0:T(8,128)(2,1)S(1)}, u32[]{:S(2)}, u32[]{:S(2)}) collective-permute-start(bf16[8,4096]{1,0:T(8,128)(2,1)S(1)} %get-tuple-element.34.refs_0_), channel_id=1, source_target_pairs={{0,2},{1,3},{2,0},{3,1},{4,6},{5,7},{6,4},{7,5},{8,10},{9,11},{10,... | collective-permute-start | bytes 196616 | tf_op jit(solution)/shard_map/ppermute | solution.py:42
  38.6 5.9 %collective-permute-start.8 = (bf16[8,4096]{1,0:T(8,128)(2,1)S(1)}, bf16[8,4096]{1,0:T(8,128)(2,1)S(1)}, u32[]{:S(2)}, u32[]{:S(2)}) collective-permute-start(bf16[8,4096]{1,0:T(8,128)(2,1)S(1)} %get-tuple-element.34.refs_0_), channel_id=1, source_target_pairs={{0,4},{1,5},{2,6},{3,7},{4,0},{5,1},{6,2},{7,3},{8,12},{9,13},{10,... | collective-permute-start | bytes 196616 | tf_op jit(solution)/shard_map/ppermute | solution.py:42
  38.6 5.9 %collective-permute-start.7 = (bf16[8,4096]{1,0:T(8,128)(2,1)S(1)}, bf16[8,4096]{1,0:T(8,128)(2,1)S(1)}, u32[]{:S(2)}, u32[]{:S(2)}) collective-permute-start(bf16[8,4096]{1,0:T(8,128)(2,1)S(1)} %get-tuple-element.34.refs_0_), channel_id=1, source_target_pairs={{0,8},{1,9},{2,10},{3,11},{4,12},{5,13},{6,14},{7,15},{8,0},{9,1},... | collective-permute-start | bytes 196616 | tf_op jit(solution)/shard_map/ppermute | solution.py:42
  42.8 4.3 %collective-permute-start.10 = (bf16[8,4096]{1,0:T(8,128)(2,1)S(1)}, bf16[8,4096]{1,0:T(8,128)(2,1)S(1)}, u32[]{:S(2)}, u32[]{:S(2)}) collective-permute-start(bf16[8,4096]{1,0:T(8,128)(2,1)S(1)} %collective-permute-done.6.refs_1_), channel_id=1, source_target_pairs={{0,2},{1,3},{2,0},{3,1},{4,6},{5,7},{6,4},{7,5},{8,10},{9,11},{10,... | collective-permute-start | bytes 196616 | tf_op jit(solution)/shard_map/ppermute | solution.py:42
  47.1 21.0 %copy-start.1 = (bf16[1,2048,512]{2,1,0:T(8,128)(2,1)S(1)}, bf16[1,2048,512]{2,1,0:T(8,128)(2,1)}, u32[]{:S(2)}) copy-start(bf16[1,2048,512]{2,1,0:T(8,128)(2,1)} %up_ref.1) | copy-start | bytes 6291460
  47.1 21.0 %copy-start = (bf16[1,2048,512]{2,1,0:T(8,128)(2,1)S(1)}, bf16[1,2048,512]{2,1,0:T(8,128)(2,1)}, u32[]{:S(2)}) copy-start(bf16[1,2048,512]{2,1,0:T(8,128)(2,1)} %gate_ref.1) | copy-start | bytes 6291460
  47.2 7.6 %collective-permute-start.12 = (bf16[6,8,4096]{2,1,0:T(8,128)(2,1)S(1)}, bf16[6,8,4096]{2,1,0:T(8,128)(2,1)S(1)}, u32[]{:S(2)}, u32[]{:S(2)}) collective-permute-start(bf16[6,8,4096]{2,1,0:T(8,128)(2,1)S(1)} %join.4.refs_0_), channel_id=1, source_target_pairs={{0,1},{1,0},{2,3},{3,2},{4,5},{5,4},{6,7},{7,6},{8,9},{9,8},{10,11... | collective-permute-start | bytes 1179656 | tf_op jit(solution)/shard_map/ppermute | solution.py:42
  47.2 6.0 %collective-permute-start.11 = (bf16[2,8,4096]{2,1,0:T(8,128)(2,1)S(1)}, bf16[2,8,4096]{2,1,0:T(8,128)(2,1)S(1)}, u32[]{:S(2)}, u32[]{:S(2)}) collective-permute-start(bf16[2,8,4096]{2,1,0:T(8,128)(2,1)S(1)} %join.5), channel_id=1, source_target_pairs={{0,2},{1,3},{2,0},{3,1},{4,6},{5,7},{6,4},{7,5},{8,10},{9,11},{10,... | collective-permute-start | bytes 393224 | tf_op jit(solution)/shard_map/ppermute | solution.py:42
  53.2 1.6 %collective-permute-start.13 = (bf16[2,8,4096]{2,1,0:T(8,128)(2,1)S(1)}, bf16[2,8,4096]{2,1,0:T(8,128)(2,1)S(1)}, u32[]{:S(2)}, u32[]{:S(2)}) collective-permute-start(bf16[2,8,4096]{2,1,0:T(8,128)(2,1)S(1)} %collective-permute-done.11.refs_1_), channel_id=1, source_target_pairs={{0,1},{1,0},{2,3},{3,2},{4,5},{5,4},{6,7},{7,6},{8,9},{9,8},{10,11... | collective-permute-start | bytes 393224 | tf_op jit(solution)/shard_map/ppermute | solution.py:42
  54.3 13.9 %copy-start.28 = (bf16[2048]{0:T(1024)(128)(2,1)S(1)}, bf16[2048]{0:T(1024)(128)(2,1)}, u32[]{:S(2)}) copy-start(bf16[2048]{0:T(1024)(128)(2,1)} %param.42) | copy-start | bytes 12292
  70.4 13.5 %all-to-all-start.2 = ((bf16[16,8,1024]{2,1,0:T(8,128)(2,1)}), bf16[16,8,1024]{2,1,0:T(8,128)(2,1)S(1)}, u32[]{:S(2)}, u32[]{:S(2)}) async-start(bf16[16,8,1024]{2,1,0:T(8,128)(2,1)} %get-tuple-element.36), calls=%async_computation.2 | async-start | bytes 524288 | tf_op jit(solution)/shard_map/all_to_all | solution.py:656
  (13 other events, 35.9 us)
